TPU v7x, 256 devices: a whole 4x4x8 slice. The times are simulated.
256 devices in a mesh: kv: 32 (over z, y), tp: 8 (over x, core).
Axes of the slice: x: 4, y: 4, z: 8, core: 2. Of those that a mesh axis runs over, the one named last changes fastest.
Arguments:
- tokens: bfloat16 [128, 4096], P(None, 'kv'), may hold values from -8 to 8, as said below
- attn_gain: float32 [4096], P('kv'), may hold values from 0.1 to 1.9
- query_weight: bfloat16 [4096, 1024], P('kv', 'tp'), may hold values from -0.09375 to 0.09375
- key_weight: bfloat16 [4096, 1024], P('kv', 'tp'), may hold values from -0.09375 to 0.09375
- value_weight: bfloat16 [4096, 2048], P('kv', 'tp'), may hold values from -0.09375 to 0.09375
- outgate_weight: bfloat16 [4096, 2048], P('kv', 'tp'), may hold values from -0.09375 to 0.09375
- code_weight: bfloat16 [4096, 16], P('kv'), may hold values from -0.09375 to 0.09375
- decay_weight: bfloat16 [16, 1024], P(None, 'tp'), may hold values from -6 to 6
- decay_bias: float32 [1024], P('tp'), may hold values from -4 to 2
- head_gain: float32 [256], replicated, may hold values from 0.1 to 1.9
- key_cache: bfloat16 [128, 64, 8, 128], P('kv', None, 'tp'), may hold values from -6 to 6
- value_cache: bfloat16 [128, 64, 8, 256], P('kv', None, 'tp'), may hold values from -6 to 6
- decay_cache: float32 [128, 64, 8, 128], P('kv', None, 'tp'), may hold values from -1.1 to 0
- carried_state: float32 [128, 8, 128, 256], P('kv', 'tp'), may hold values from -24 to 24
- lengths: int32 [128], P('kv'), may hold values from 1 to 64, 3328 in all
- output_weight: bfloat16 [2048, 4096], P('tp', 'kv'), may hold values from -0.125 to 0.125
- mlp_gain: float32 [4096], P('kv'), may hold values from 0.1 to 1.9
- gate_weight: bfloat16 [4096, 11008], P('kv', 'tp'), may hold values from -0.09375 to 0.09375
- up_weight: bfloat16 [4096, 11008], P('kv', 'tp'), may hold values from -0.09375 to 0.09375
- down_weight: bfloat16 [11008, 4096], P('tp', 'kv'), may hold values from -0.0546875 to 0.0546875
Outputs:
- layer_out: bfloat16 [128, 4096], P(None, 'kv')
- new_keys: bfloat16 [128, 8, 128], P('kv', 'tp')
- new_values: bfloat16 [128, 8, 256], P('kv', 'tp')
Inputs may be any that keep to these rules, and one draw needn't show every extreme that they name: `tokens`: the features of a row have unlike scales. Sequence b's new token comes right after its lengths[b] live positions; positions from lengths[b] on take no part.
All inputs are finite; a program needn't handle non-finite values. No bound on the sum of `lengths` on one device may be relied on, other than what follows from the above.
Results may differ from a plain program's by a relative error of at most 0.025.
Values may be sent and summed in bfloat16 or wider, within the bound.
No kernel may reach another device: no remote copies, remote signals or barrier semaphores. Data moves between devices by JAX's collectives and lax.ppermute only.
A program may use at most 64 MiB of HBM per device.

v0:
```python
import jax
import jax.numpy as jnp
from jax import lax
from jax.experimental import pallas as pl
from jax.experimental.pallas import tpu as pltpu
from jax.sharding import Mesh
from jax.sharding import PartitionSpec as P

WIDTH = 4096
EPS = 1e-06
GATE_TEMP = 16.0
KV = ("z", "y")
TP = ("x", "c")
F32 = jnp.float32
BF16 = jnp.bfloat16
FIRST = 512
CODE_AT = 256
SQUARE_AT = 272
TOKENS_AT = 256
GAIN_AT = 384
SENT = 400
UNITS = 1376
SECOND = 1408


def kernel(body, outs, args, fetched=()):
    count, more = len(args), len(fetched)

    def whole(*refs):
        arg_refs, from_refs = refs[:count], refs[count : count + more]
        out_refs = refs[count + more : -1] if more else refs[count:]
        copies = [
            pltpu.make_async_copy(
                source, out_refs[out].at[pl.ds(row, source.shape[0])], refs[-1].at[k]
            )
            for k, (source, (_, out, row)) in enumerate(zip(from_refs, fetched))
        ]
        for copy in copies:
            copy.start()
        body(*arg_refs, *out_refs)
        for copy in copies:
            copy.wait()

    return pl.pallas_call(
        whole,
        out_shape=tuple(pltpu.VMEM(*out) for out in outs),
        in_specs=[pl.BlockSpec(memory_space=pltpu.VMEM)] * count + [pl.BlockSpec(memory_space=pl.ANY)] * more,
        out_specs=[pl.BlockSpec(memory_space=pltpu.VMEM)] * len(outs),
        scratch_shapes=[pltpu.SemaphoreType.DMA((more,))] if more else [],
        compiler_params=pltpu.CompilerParams(vmem_limit_bytes=8 << 20),
    )(*args, *(in_hbm(array) for array, _, _ in fetched))


def in_hbm(x):
    return pltpu.with_memory_space_constraint(x, pltpu.HBM)


def store_shares(out_ref, low, high, at=0):
    rows, width = low.shape
    low = low.reshape(rows // 8, 8, width)
    high = high.reshape(rows // 8, 8, width)
    first = lax.broadcasted_iota(jnp.int32, low.shape, 1) < 4
    out_ref[:, 0, :, at : at + width] = jnp.where(first, low, pltpu.roll(high, 4, 1)).astype(BF16)
    out_ref[:, 1, :, at : at + width] = jnp.where(first, pltpu.roll(low, 4, 1), high).astype(BF16)


def dot(a, b, dims=((1,), (0,)), **kw):
    return lax.dot_general(a, b, (dims, ((), ())), preferred_element_type=F32, **kw)


def project_body(tok_ref, gain_ref, q_ref, k_ref, v_ref, g_ref, code_ref, mlp_gain_ref, out_ref, sent_ref, *_):
    part = mlp_gain_ref[...]
    rows = []
    for _ in range(3):
        rows.append(rounded(part))
        part = part - rows[-1]
    rows = jnp.concatenate([*rows, jnp.zeros((SENT - GAIN_AT - 3, 128), F32)], axis=0)
    sent_ref[GAIN_AT:SENT, :] = rows.astype(BF16)
    tok = tok_ref[...].astype(F32)
    scaled = (tok * gain_ref[...]).astype(BF16)
    squares = jnp.sum(tok * tok, axis=1, keepdims=True)
    code = dot(scaled, code_ref[...], ((1,), (1,)))
    lane = lax.broadcasted_iota(jnp.int32, (128, 256), 1)
    tail = jnp.concatenate([code, jnp.zeros((128, 240), F32)], axis=1)
    tail = jnp.where(lane == SQUARE_AT - CODE_AT, squares, tail)
    out_gate = dot(scaled, g_ref[...])
    head = jnp.concatenate([dot(scaled, q_ref[...]), dot(scaled, k_ref[...])], axis=1)
    store_shares(out_ref, head, out_gate)
    store_shares(out_ref, dot(scaled, v_ref[...]), tail, 256)


def rounded(x):
    return x.astype(BF16).astype(F32)


def attend_body(
    got_ref, dw_ref, bias_ref, hg_ref, len_ref, decay_hbm, key_hbm, value_hbm, state_hbm,
    heads_ref, nk_ref, nv_ref, decay_ref, key_ref, value_ref, state_ref, sems,
):
    sources = (decay_hbm, key_hbm, value_hbm, state_hbm)
    targets = (decay_ref, key_ref, value_ref, state_ref)
    copies = [pltpu.make_async_copy(a, b, sems.at[k]) for k, (a, b) in enumerate(zip(sources, targets))]
    for copy in copies:
        copy.start()
    total = jnp.sum(got_ref[...].astype(F32), axis=0)
    squares = jnp.broadcast_to(total[:, SQUARE_AT : SQUARE_AT + 1], (8, 128))
    inv_high = lax.rsqrt(squares / WIDTH + EPS)
    inv_low = pltpu.roll(inv_high, 4, 0)
    twice = lambda x: jnp.concatenate([x, x], axis=1)
    queries = rounded(total[:, 0:128] * inv_low * 128 ** (-0.5))
    keys = (total[:, 128:256] * inv_low).astype(BF16)
    values = (total[:, 256:512] * twice(inv_low)).astype(BF16)
    out_gate = pltpu.roll(rounded(total[:, 0:256] * twice(inv_high)), 4, 0)
    code = (total[:, CODE_AT : CODE_AT + 128] * inv_high).astype(BF16)[:, 0:16]
    pre = pltpu.roll(dot(code, dw_ref[...]) + bias_ref[...], 4, 0)
    log_sig = jnp.minimum(pre, 0.0) - jnp.log1p(jnp.exp(-jnp.abs(pre)))
    decayed = queries * jnp.exp(log_sig / GATE_TEMP)
    own = jnp.sum(queries * keys.astype(F32), axis=1, keepdims=True)
    row = lax.broadcasted_iota(jnp.int32, (64, 64), 0)
    col = lax.broadcasted_iota(jnp.int32, (64, 64), 1)
    later = (col > row).astype(F32)
    position = lax.broadcasted_iota(jnp.int32, (64, 128), 0)
    copies[0].wait()
    live = [position < len_ref[:, b : b + 1] for b in range(4)]
    kept = [jnp.where(live[b], decay_ref[b], 0.0) for b in range(4)]
    sums = dot(later, jnp.concatenate(kept, axis=1), precision=lax.Precision.HIGHEST)
    totals = jnp.concatenate([jnp.sum(k, axis=0, keepdims=True) for k in kept], axis=0)
    carry = decayed[0:4] * jnp.exp(totals)
    columns = jnp.concatenate([carry, carry], axis=0).T
    for copy in copies[1:]:
        copy.wait()
    mixed = []
    for b in range(4):
        keyed = key_ref[b].astype(F32) * jnp.exp(sums[:, 128 * b : 128 * b + 128])
        scores = jnp.sum(jnp.where(live[b], keyed * decayed[b : b + 1], 0.0), axis=1, keepdims=True)
        within = jnp.sum(rounded(scores) * value_ref[b].astype(F32), axis=0, keepdims=True)
        carried = jnp.sum(columns[:, b : b + 1] * state_ref[b], axis=0, keepdims=True)
        mixed.append(carried + within)
    mixed = jnp.concatenate(mixed, axis=0) + own[0:4] * values[0:4].astype(F32)
    scale = lax.rsqrt(jnp.mean(mixed * mixed, axis=1, keepdims=True) + EPS)
    gate = out_gate[0:4]
    heads_ref[...] = (mixed * scale * hg_ref[...] * (gate / (1.0 + jnp.exp(-gate)))).astype(BF16)
    nk_ref[...] = keys[0:4]
    nv_ref[...] = values[0:4]


def sequences_of(y, shape, dim):
    place = lax.broadcasted_iota(jnp.int32, shape, dim)
    group = place // 32
    owner = jnp.where(group == 0, y, jnp.where(group == 1, y + 3, jnp.where(group == 2, y + 1, y + 2))) % 4
    return (place % 32) // 4 * 16 + owner * 4 + place % 4


def chosen(condition):
    return jnp.where(condition, 1.0, 0.0).astype(BF16)


def lift_body(mine_ref, after_ref, before_ref, across_ref, *refs):
    sent_refs, weight_refs, (mid_ref, out_ref) = refs[:4], refs[4:8], refs[8:]
    attended = (mine_ref[...].astype(F32) + across_ref[...].astype(F32)) + (
        after_ref[...].astype(F32) + before_ref[...].astype(F32)
    )
    own = sequences_of(lax.axis_index("y"), (32, 128), 0)
    pick = chosen(own == lax.broadcasted_iota(jnp.int32, (32, 128), 1))
    tok = jnp.concatenate([dot(pick, ref[TOKENS_AT:GAIN_AT, :]) for ref in sent_refs], axis=1)
    middle = (tok + attended).astype(BF16)
    mid = middle.astype(F32)
    scaled = []
    for k, ref in enumerate(sent_refs):
        mid_ref[k] = middle[:, 128 * k : 128 * k + 128]
        gain = jnp.sum(ref[GAIN_AT:SENT, :].astype(F32), axis=0, keepdims=True)
        scaled.append((mid[:, 128 * k : 128 * k + 128] * gain).astype(BF16))
    squares = jnp.sum(mid * mid, axis=1, keepdims=True)

    def product(at, size):
        return sum(
            dot(part, ref[at : at + size, :], ((1,), (1,))) for part, ref in zip(scaled, weight_refs)
        )

    for at, width in ((0, 512), (512, 512), (1024, 384)):
        real = min(width, UNITS - at)
        low = product(at, real)
        high = product(UNITS + at, real)
        if real < width:
            pad = jnp.broadcast_to(squares, (32, width - real))
            low = jnp.concatenate([low, pad], axis=1)
            high = jnp.concatenate([high, pad], axis=1)
        store_shares(out_ref, low, high, at)


def hidden_body(got_ref, out_ref):
    total = jnp.sum(got_ref[...].astype(F32), axis=0)
    inv = lax.rsqrt(total[0:4, UNITS : UNITS + 1] / WIDTH + EPS)
    gate = total[0:4] * inv
    up = pltpu.roll(total, 4, 0)[0:4] * inv
    out_ref[...] = (gate / (1.0 + jnp.exp(-gate)) * up).astype(BF16)


def down_body(hidden_ref, down_ref, *refs):
    mid_refs, (out_ref, mid_ref) = refs[:4], refs[4:]
    out_ref[...] = dot(hidden_ref[:, 0:UNITS], down_ref[...]).astype(BF16)
    whose = sequences_of(lax.axis_index("y"), (128, 128), 1)
    place = chosen(whose == lax.broadcasted_iota(jnp.int32, (128, 128), 0))
    mids = jnp.concatenate([ref[...] for ref in mid_refs], axis=0)
    mid_ref[...] = dot(place, mids).astype(BF16)


def out_body(heads_ref, *refs):
    sent_refs, out_ref = refs[:4], refs[4]
    for k, ref in enumerate(sent_refs):
        out_ref[:, 128 * k : 128 * k + 128] = dot(heads_ref[...], ref[0:TOKENS_AT, :]).astype(BF16)


def moved(x, axis, shift):
    length = lax.axis_size(axis)
    return lax.ppermute(x, axis, [(i, (i + shift) % length) for i in range(length)])


def tp_parts(mine):
    pair = (mine.astype(F32) + moved(mine, "c", 1).astype(F32)).astype(BF16)
    return (pair, *(moved(pair, "x", k) for k in (1, 3, 2)))


def to_all(x, axes):
    devices = lax.axis_size(axes)
    copies = jnp.broadcast_to(x[None], (devices, *x.shape))
    got = lax.all_to_all(copies, axes, 0, 0, tiled=True)
    return got.reshape(devices * x.shape[0], x.shape[1])


def shares(x, axes):
    return lax.all_to_all(x.reshape(-1, 8, x.shape[-1]), axes, 0, 0, tiled=True)


def along_y(x):
    got = [x]
    for k in (1, 3, 2):
        got.append(moved(x, "y", k))
    return tuple(got)


def on_device(
    tokens,
    attn_gain,
    query_weight,
    key_weight,
    value_weight,
    outgate_weight,
    code_weight,
    decay_weight,
    decay_bias,
    head_gain,
    key_cache,
    value_cache,
    decay_cache,
    carried_state,
    lengths,
    output_weight,
    mlp_gain,
    gate_weight,
    up_weight,
    down_weight,
):
    seqs = key_cache.shape[0]
    read = (tokens, attn_gain[None], query_weight, key_weight, value_weight, outgate_weight, code_weight.T)
    small = (decay_weight, decay_bias[None], head_gain[None], lengths[None])
    first, sent, lifting, *small = kernel(
        project_body,
        [
            ((32 // 2, 2, 8, FIRST), BF16),
            ((SENT, 128), BF16),
            ((2 * UNITS, 128), BF16),
            *((a.shape, a.dtype) for a in small),
        ],
        [in_hbm(a) for a in (*read, mlp_gain[None])],
        (
            (output_weight, 1, 0),
            (tokens, 1, TOKENS_AT),
            (gate_weight.T, 2, 0),
            (up_weight.T, 2, UNITS),
            *((a, 3 + k, 0) for k, a in enumerate(small)),
        ),
    )
    sent = along_y(sent)
    lifting = along_y(lifting)
    caches = (decay_cache[:, :, 0], key_cache[:, :, 0], value_cache[:, :, 0], carried_state[:, 0])
    heads, new_keys, new_values = pl.pallas_call(
        attend_body,
        out_shape=(pltpu.VMEM((seqs, 256), BF16), pltpu.VMEM((seqs, 128), BF16), pltpu.VMEM((seqs, 256), BF16)),
        in_specs=[pl.BlockSpec(memory_space=pltpu.VMEM)] * 5 + [pl.BlockSpec(memory_space=pl.ANY)] * 4,
        out_specs=[pl.BlockSpec(memory_space=pltpu.VMEM)] * 3,
        scratch_shapes=[
            *(pltpu.VMEM(a.shape, a.dtype) for a in caches),
            pltpu.SemaphoreType.DMA((4,)),
        ],
        compiler_params=pltpu.CompilerParams(vmem_limit_bytes=8 << 20),
        name="attend",
    )(shares(first, KV), *small, *map(in_hbm, caches))
    (attended,) = kernel(out_body, [((32, 512), BF16)], (to_all(heads, "z"), *sent))
    middle, second = kernel(
        lift_body, [((4, 32, 128), BF16), ((4, 2, 8, SECOND), BF16)], (*tp_parts(attended), *sent, *lifting)
    )
    (hidden,) = kernel(hidden_body, [((seqs, SECOND), BF16)], (shares(second, "z"),))
    middles = (middle[0], moved(middle[2], "y", 1), moved(middle[1], "y", 3), moved(middle[3], "y", 2))
    lifted, middle = kernel(
        down_body, [((128, 128), BF16), ((128, 128), BF16)], (to_all(hidden, KV), down_weight, *middles)
    )
    mine, after, before, across = (part.astype(F32) for part in tp_parts(lifted))
    layer_out = (middle.astype(F32) + ((mine + across) + (after + before))).astype(BF16)
    return (layer_out, new_keys[:, None], new_values[:, None])


def solution(mesh):
    axes = Mesh(mesh.devices.reshape(8, 4, 4, 2), ("z", "y", "x", "c"))
    in_specs = (
        P(None, KV),
        P(KV),
        P(KV, TP),
        P(KV, TP),
        P(KV, TP),
        P(KV, TP),
        P(KV, None),
        P(None, TP),
        P(TP),
        P(),
        P(KV, None, TP, None),
        P(KV, None, TP, None),
        P(KV, None, TP, None),
        P(KV, TP, None, None),
        P(KV),
        P(TP, KV),
        P(KV),
        P(KV, TP),
        P(KV, TP),
        P(TP, KV),
    )
    out_specs = (P(None, KV), P(KV, TP, None), P(KV, TP, None))
    return jax.shard_map(
        on_device, mesh=axes, in_specs=in_specs, out_specs=out_specs, check_vma=False
    )
```

profile of v0, /device:TPU:1, one launch (start us, length us, event | category | flops | bytes accessed | tf_op | source)
XLA Modules:
  0.0 123.4 jit_solution(4410776008010388074)
XLA Ops:
  0.6 2.9 %shard_map.211 = (bf16[16,2,8,512]{3,2,1,0:T(8,128)(2,1)}, bf16[400,128]{1,0:T(8,128)(2,1)S(1)}, bf16[2752,128]{1,0:T(8,128)(2,1)S(1)}, bf16[16,128]{1,0:T(8,128...) custom-call(bf16[128,128]{1,0:T(8,128)(2,1)} %refs_9_.1, f32[1,128]{1,0:T(1,128)} %bitcast.35, ...), custom_call_target="tpu_custom_call" | custom-call | tf_op jit(solution)/shard_map/pallas_call | solution.py:44
  3.5 12.0 %all-to-all-start = ((bf16[32,8,512]{2,1,0:T(8,128)(2,1)}), bf16[32,8,512]{2,1,0:T(8,128)(2,1)S(1)}, u32[]{:S(2)}, u32[]{:S(2)}) async-start(bf16[32,8,512]{2,1,0:T(8,128)(2,1)} %bitcast.8), calls=%async_computation | async-start | bytes 524288 | tf_op jit(solution)/shard_map/all_to_all | solution.py:232
  15.6 2.8 %collective-permute-start.9 = (bf16[2752,128]{1,0:T(8,128)(2,1)S(1)}, bf16[2752,128]{1,0:T(8,128)(2,1)S(1)}, u32[]{:S(2)}, u32[]{:S(2)}) collective-permute-start(bf16[2752,128]{1,0:T(8,128)(2,1)S(1)} %get-tuple-element.24.refs_8_), channel_id=1, source_target_pairs={{0,16},{8,24},{16,0},{24,8},{1,17},{9,25},{17,1},{25,9},{2,18},{10... | collective-permute-start | bytes 2113544 | tf_op jit(solution)/shard_map/ppermute | solution.py:216
  18.4 0.9 collective-permute-start.8
  19.3 0.6 collective-permute-start.7
  19.9 0.6 collective-permute-start.2
  20.5 2.1 %collective-permute-start.1 = (bf16[400,128]{1,0:T(8,128)(2,1)S(1)}, bf16[400,128]{1,0:T(8,128)(2,1)S(1)}, u32[]{:S(2)}, u32[]{:S(2)}) collective-permute-start(bf16[400,128]{1,0:T(8,128)(2,1)S(1)} %get-tuple-element.23.refs_1_.refs_4_), channel_id=1, source_target_pairs={{0,24},{8,0},{16,8},{24,16},{1,25},{9,1},{17,9},{25,17},{2,26},{10... | collective-permute-start | bytes 307208 | tf_op jit(solution)/shard_map/ppermute | solution.py:216
  22.6 30.8 %collective-permute-done.2.refs_4_.refs_7_ = bf16[400,128]{1,0:T(8,128)(2,1)S(1)} collective-permute-done((bf16[400,128]{1,0:T(8,128)(2,1)S(1)}, bf16[400,128]{1,0:T(8,128)(2,1)S(1)}, u32[]{:S(2)}, u32[]{:S(2)}) %collective-permute-start.2) | collective-permute-done | bytes 102432 | tf_op jit(solution)/shard_map/ppermute | solution.py:216
  53.4 1.2 %collective-permute-start = (bf16[400,128]{1,0:T(8,128)(2,1)S(1)}, bf16[400,128]{1,0:T(8,128)(2,1)S(1)}, u32[]{:S(2)}, u32[]{:S(2)}) collective-permute-start(bf16[400,128]{1,0:T(8,128)(2,1)S(1)} %get-tuple-element.23.refs_1_.refs_4_), channel_id=1, source_target_pairs={{0,8},{8,16},{16,24},{24,0},{1,9},{9,17},{17,25},{25,1},{2,10},{10... | collective-permute-start | bytes 307208 | tf_op jit(solution)/shard_map/ppermute | solution.py:216
  54.7 1.7 %attend.1 = (bf16[4,256]{1,0:T(4,128)(2,1)S(1)}, bf16[4,128]{1,0:T(4,128)(2,1)S(1)}, bf16[4,256]{1,0:T(4,128)(2,1)S(1)}) custom-call(bf16[32,8,512]{2,1,0:T(8,128)(2,1)S(1)} %all-to-all-done.got_ref, bf16[16,128]{1,0:T(8,128)(2,1)S(1)} %get-tuple-element.18.dw_ref, f32[1,128]{1,0:T(1,128)S(1)} %get-tuple-element.19.bias_ref, ...), custom_call_target="tpu_custom_call" | custom-call | tf_op jit(solution)/shard_map/attend/pallas_call | solution.py:287
  56.4 12.9 %all_to_all.20 = bf16[8,4,256]{2,1,0:T(4,128)(2,1)S(1)} all-to-all(bf16[8,4,256]{2,1,0:T(4,128)(2,1)S(1)} %broadcast_in_dim.38), channel_id=1, replica_groups=mesh['z'=8,'y'=4,'x'=4,'c'=2] {'z'}, dimensions={0} | all-to-all | bytes 32768 | tf_op jit(solution)/shard_map/all_to_all | solution.py:227
  69.6 3.6 %collective-permute-start.3 = (bf16[32,512]{1,0:T(8,128)(2,1)S(1)}, bf16[32,512]{1,0:T(8,128)(2,1)S(1)}, u32[]{:S(2)}, u32[]{:S(2)}) collective-permute-start(bf16[32,512]{1,0:T(8,128)(2,1)S(1)} %shard_map.212), channel_id=1, source_target_pairs={{0,1},{1,0},{2,3},{3,2},{4,5},{5,4},{6,7},{7,6},{8,9},{9,8},{10,11... | collective-permute-start | bytes 98312 | tf_op jit(solution)/shard_map/ppermute | solution.py:216
  73.2 0.9 collective-permute-done.3
  74.1 2.8 %collective-permute-start.6 = (bf16[32,512]{1,0:T(8,128)(2,1)S(1)}, bf16[32,512]{1,0:T(8,128)(2,1)S(1)}, u32[]{:S(2)}, u32[]{:S(2)}) collective-permute-start(bf16[32,512]{1,0:T(8,128)(2,1)S(1)} %add_convert_fusion.2.refs_0_), channel_id=1, source_target_pairs={{0,4},{2,6},{4,0},{6,2},{1,5},{3,7},{5,1},{7,3},{8,12},{10,14},{12... | collective-permute-start | bytes 98312 | tf_op jit(solution)/shard_map/ppermute | solution.py:216
  76.9 0.9 collective-permute-start.5
  77.8 0.7 collective-permute-done.6.refs_3_
  78.4 1.2 collective-permute-start.4
  79.7 2.7 %collective-permute-done.4.refs_1_ = bf16[32,512]{1,0:T(8,128)(2,1)S(1)} collective-permute-done((bf16[32,512]{1,0:T(8,128)(2,1)S(1)}, bf16[32,512]{1,0:T(8,128)(2,1)S(1)}, u32[]{:S(2)}, u32[]{:S(2)}) %collective-permute-start.4) | collective-permute-done | bytes 32800 | tf_op jit(solution)/shard_map/ppermute | solution.py:216
  82.4 1.2 shard_map.213
  83.6 10.9 %all_to_all.21.refs_0_ = bf16[8,8,1408]{2,1,0:T(8,128)(2,1)S(1)} all-to-all(bf16[8,8,1408]{2,1,0:T(8,128)(2,1)S(1)} %bitcast.26), channel_id=1, replica_groups=mesh['z'=8,'y'=4,'x'=4,'c'=2] {'z'}, dimensions={0} | all-to-all | bytes 360448 | tf_op jit(solution)/shard_map/all_to_all | solution.py:232
  94.6 0.8 broadcast_in_dim.39
  95.5 3.9 %all-to-all-start.3 = ((bf16[32,4,1408]{2,1,0:T(4,128)(2,1)}), bf16[32,4,1408]{2,1,0:T(4,128)(2,1)S(1)}, u32[]{:S(2)}, u32[]{:S(2)}) async-start(bf16[32,4,1408]{2,1,0:T(4,128)(2,1)} %broadcast_in_dim.39), calls=%async_computation.3 | async-start | bytes 720896 | tf_op jit(solution)/shard_map/all_to_all | solution.py:227
  99.4 2.7 %collective-permute-start.12 = (bf16[32,128]{1,0:T(8,128)(2,1)S(1)}, bf16[32,128]{1,0:T(8,128)(2,1)S(1)}, u32[]{:S(2)}, u32[]{:S(2)}) collective-permute-start(bf16[32,128]{1,0:T(8,128)(2,1)S(1)} %get-tuple-element.31), channel_id=1, source_target_pairs={{0,16},{8,24},{16,0},{24,8},{1,17},{9,25},{17,1},{25,9},{2,18},{10... | collective-permute-start | bytes 24584 | tf_op jit(solution)/shard_map/ppermute | solution.py:216
  102.1 0.9 collective-permute-start.11
  103.0 0.6 collective-permute-start.10
  103.5 7.4 %all-to-all-done.3 = bf16[32,4,1408]{2,1,0:T(4,128)(2,1)S(1)} async-done(((bf16[32,4,1408]{2,1,0:T(4,128)(2,1)}), bf16[32,4,1408]{2,1,0:T(4,128)(2,1)S(1)}, u32[]{:S(2)}, u32[]{:S(2)}) %all-to-all-start.3) | async-done | bytes 360480 | tf_op jit(solution)/shard_map/all_to_all | solution.py:227
  111.3 4.8 %collective-permute-start.13 = (bf16[128,128]{1,0:T(8,128)(2,1)S(1)}, bf16[128,128]{1,0:T(8,128)(2,1)S(1)}, u32[]{:S(2)}, u32[]{:S(2)}) collective-permute-start(bf16[128,128]{1,0:T(8,128)(2,1)S(1)} %get-tuple-element.28), channel_id=1, source_target_pairs={{0,1},{1,0},{2,3},{3,2},{4,5},{5,4},{6,7},{7,6},{8,9},{9,8},{10,11... | collective-permute-start | bytes 98312 | tf_op jit(solution)/shard_map/ppermute | solution.py:216
  116.1 0.9 collective-permute-done.13
  117.0 1.4 %collective-permute-start.16 = (bf16[128,128]{1,0:T(8,128)(2,1)S(1)}, bf16[128,128]{1,0:T(8,128)(2,1)S(1)}, u32[]{:S(2)}, u32[]{:S(2)}) collective-permute-start(bf16[128,128]{1,0:T(8,128)(2,1)S(1)} %add_convert_fusion.1), channel_id=1, source_target_pairs={{0,6},{2,0},{4,2},{6,4},{1,7},{3,1},{5,3},{7,5},{8,14},{10,8},{12,... | collective-permute-start | bytes 98312 | tf_op jit(solution)/shard_map/ppermute | solution.py:216
  118.5 1.5 %collective-permute-start.14 = (bf16[128,128]{1,0:T(8,128)(2,1)S(1)}, bf16[128,128]{1,0:T(8,128)(2,1)S(1)}, u32[]{:S(2)}, u32[]{:S(2)}) collective-permute-start(bf16[128,128]{1,0:T(8,128)(2,1)S(1)} %add_convert_fusion.1), channel_id=1, source_target_pairs={{0,4},{2,6},{4,0},{6,2},{1,5},{3,7},{5,1},{7,3},{8,12},{10,14},{12... | collective-permute-start | bytes 98312 | tf_op jit(solution)/shard_map/ppermute | solution.py:216
  121.2 1.1 collective-permute-done.15
  122.8 0.6 add_convert_fusion
  (26 shorter events, 2.4 us)
Async XLA Ops:
  3.5 51.1 %all-to-all-start = ((bf16[32,8,512]{2,1,0:T(8,128)(2,1)}), bf16[32,8,512]{2,1,0:T(8,128)(2,1)S(1)}, u32[]{:S(2)}, u32[]{:S(2)}) async-start(bf16[32,8,512]{2,1,0:T(8,128)(2,1)} %bitcast.8), calls=%async_computation | async-start | bytes 524288 | tf_op jit(solution)/shard_map/all_to_all | solution.py:232
  15.6 66.8 %collective-permute-start.9 = (bf16[2752,128]{1,0:T(8,128)(2,1)S(1)}, bf16[2752,128]{1,0:T(8,128)(2,1)S(1)}, u32[]{:S(2)}, u32[]{:S(2)}) collective-permute-start(bf16[2752,128]{1,0:T(8,128)(2,1)S(1)} %get-tuple-element.24.refs_8_), channel_id=1, source_target_pairs={{0,16},{8,24},{16,0},{24,8},{1,17},{9,25},{17,1},{25,9},{2,18},{10... | collective-permute-start | bytes 2113544 | tf_op jit(solution)/shard_map/ppermute | solution.py:216
  18.4 64.0 %collective-permute-start.8 = (bf16[2752,128]{1,0:T(8,128)(2,1)S(1)}, bf16[2752,128]{1,0:T(8,128)(2,1)S(1)}, u32[]{:S(2)}, u32[]{:S(2)}) collective-permute-start(bf16[2752,128]{1,0:T(8,128)(2,1)S(1)} %get-tuple-element.24.refs_8_), channel_id=1, source_target_pairs={{0,24},{8,0},{16,8},{24,16},{1,25},{9,1},{17,9},{25,17},{2,26},{10... | collective-permute-start | bytes 2113544 | tf_op jit(solution)/shard_map/ppermute | solution.py:216
  19.3 63.1 %collective-permute-start.7 = (bf16[2752,128]{1,0:T(8,128)(2,1)S(1)}, bf16[2752,128]{1,0:T(8,128)(2,1)S(1)}, u32[]{:S(2)}, u32[]{:S(2)}) collective-permute-start(bf16[2752,128]{1,0:T(8,128)(2,1)S(1)} %get-tuple-element.24.refs_8_), channel_id=1, source_target_pairs={{0,8},{8,16},{16,24},{24,0},{1,9},{9,17},{17,25},{25,1},{2,10},{10... | collective-permute-start | bytes 2113544 | tf_op jit(solution)/shard_map/ppermute | solution.py:216
  19.9 33.5 %collective-permute-start.2 = (bf16[400,128]{1,0:T(8,128)(2,1)S(1)}, bf16[400,128]{1,0:T(8,128)(2,1)S(1)}, u32[]{:S(2)}, u32[]{:S(2)}) collective-permute-start(bf16[400,128]{1,0:T(8,128)(2,1)S(1)} %get-tuple-element.23.refs_1_.refs_4_), channel_id=1, source_target_pairs={{0,16},{8,24},{16,0},{24,8},{1,17},{9,25},{17,1},{25,9},{2,18},{10... | collective-permute-start | bytes 307208 | tf_op jit(solution)/shard_map/ppermute | solution.py:216
  20.5 48.9 %collective-permute-start.1 = (bf16[400,128]{1,0:T(8,128)(2,1)S(1)}, bf16[400,128]{1,0:T(8,128)(2,1)S(1)}, u32[]{:S(2)}, u32[]{:S(2)}) collective-permute-start(bf16[400,128]{1,0:T(8,128)(2,1)S(1)} %get-tuple-element.23.refs_1_.refs_4_), channel_id=1, source_target_pairs={{0,24},{8,0},{16,8},{24,16},{1,25},{9,1},{17,9},{25,17},{2,26},{10... | collective-permute-start | bytes 307208 | tf_op jit(solution)/shard_map/ppermute | solution.py:216
  53.4 16.0 %collective-permute-start = (bf16[400,128]{1,0:T(8,128)(2,1)S(1)}, bf16[400,128]{1,0:T(8,128)(2,1)S(1)}, u32[]{:S(2)}, u32[]{:S(2)}) collective-permute-start(bf16[400,128]{1,0:T(8,128)(2,1)S(1)} %get-tuple-element.23.refs_1_.refs_4_), channel_id=1, source_target_pairs={{0,8},{8,16},{16,24},{24,0},{1,9},{9,17},{17,25},{25,1},{2,10},{10... | collective-permute-start | bytes 307208 | tf_op jit(solution)/shard_map/ppermute | solution.py:216
  69.6 4.5 %collective-permute-start.3 = (bf16[32,512]{1,0:T(8,128)(2,1)S(1)}, bf16[32,512]{1,0:T(8,128)(2,1)S(1)}, u32[]{:S(2)}, u32[]{:S(2)}) collective-permute-start(bf16[32,512]{1,0:T(8,128)(2,1)S(1)} %shard_map.212), channel_id=1, source_target_pairs={{0,1},{1,0},{2,3},{3,2},{4,5},{5,4},{6,7},{7,6},{8,9},{9,8},{10,11... | collective-permute-start | bytes 98312 | tf_op jit(solution)/shard_map/ppermute | solution.py:216
  74.1 4.4 %collective-permute-start.6 = (bf16[32,512]{1,0:T(8,128)(2,1)S(1)}, bf16[32,512]{1,0:T(8,128)(2,1)S(1)}, u32[]{:S(2)}, u32[]{:S(2)}) collective-permute-start(bf16[32,512]{1,0:T(8,128)(2,1)S(1)} %add_convert_fusion.2.refs_0_), channel_id=1, source_target_pairs={{0,4},{2,6},{4,0},{6,2},{1,5},{3,7},{5,1},{7,3},{8,12},{10,14},{12... | collective-permute-start | bytes 98312 | tf_op jit(solution)/shard_map/ppermute | solution.py:216
  76.9 2.8 %collective-permute-start.5 = (bf16[32,512]{1,0:T(8,128)(2,1)S(1)}, bf16[32,512]{1,0:T(8,128)(2,1)S(1)}, u32[]{:S(2)}, u32[]{:S(2)}) collective-permute-start(bf16[32,512]{1,0:T(8,128)(2,1)S(1)} %add_convert_fusion.2.refs_0_), channel_id=1, source_target_pairs={{0,6},{2,0},{4,2},{6,4},{1,7},{3,1},{5,3},{7,5},{8,14},{10,8},{12,... | collective-permute-start | bytes 98312 | tf_op jit(solution)/shard_map/ppermute | solution.py:216
  78.4 4.0 %collective-permute-start.4 = (bf16[32,512]{1,0:T(8,128)(2,1)S(1)}, bf16[32,512]{1,0:T(8,128)(2,1)S(1)}, u32[]{:S(2)}, u32[]{:S(2)}) collective-permute-start(bf16[32,512]{1,0:T(8,128)(2,1)S(1)} %add_convert_fusion.2.refs_0_), channel_id=1, source_target_pairs={{0,2},{2,4},{4,6},{6,0},{1,3},{3,5},{5,7},{7,1},{8,10},{10,12},{12... | collective-permute-start | bytes 98312 | tf_op jit(solution)/shard_map/ppermute | solution.py:216
  95.5 15.4 %all-to-all-start.3 = ((bf16[32,4,1408]{2,1,0:T(4,128)(2,1)}), bf16[32,4,1408]{2,1,0:T(4,128)(2,1)S(1)}, u32[]{:S(2)}, u32[]{:S(2)}) async-start(bf16[32,4,1408]{2,1,0:T(4,128)(2,1)} %broadcast_in_dim.39), calls=%async_computation.3 | async-start | bytes 720896 | tf_op jit(solution)/shard_map/all_to_all | solution.py:227
  99.4 11.6 %collective-permute-start.12 = (bf16[32,128]{1,0:T(8,128)(2,1)S(1)}, bf16[32,128]{1,0:T(8,128)(2,1)S(1)}, u32[]{:S(2)}, u32[]{:S(2)}) collective-permute-start(bf16[32,128]{1,0:T(8,128)(2,1)S(1)} %get-tuple-element.31), channel_id=1, source_target_pairs={{0,16},{8,24},{16,0},{24,8},{1,17},{9,25},{17,1},{25,9},{2,18},{10... | collective-permute-start | bytes 24584 | tf_op jit(solution)/shard_map/ppermute | solution.py:216
  102.1 8.9 %collective-permute-start.11 = (bf16[32,128]{1,0:T(8,128)(2,1)S(1)}, bf16[32,128]{1,0:T(8,128)(2,1)S(1)}, u32[]{:S(2)}, u32[]{:S(2)}) collective-permute-start(bf16[32,128]{1,0:T(8,128)(2,1)S(1)} %get-tuple-element.32), channel_id=1, source_target_pairs={{0,24},{8,0},{16,8},{24,16},{1,25},{9,1},{17,9},{25,17},{2,26},{10... | collective-permute-start | bytes 24584 | tf_op jit(solution)/shard_map/ppermute | solution.py:216
  103.0 8.1 %copy-start = (bf16[1376,128]{1,0:T(8,128)(2,1)S(1)}, bf16[1376,128]{1,0:T(8,128)(2,1)}, u32[]{:S(2)}) copy-start(bf16[1376,128]{1,0:T(8,128)(2,1)} %refs_1_.1) | copy-start | bytes 1056772
  103.0 8.1 %collective-permute-start.10 = (bf16[32,128]{1,0:T(8,128)(2,1)S(1)}, bf16[32,128]{1,0:T(8,128)(2,1)S(1)}, u32[]{:S(2)}, u32[]{:S(2)}) collective-permute-start(bf16[32,128]{1,0:T(8,128)(2,1)S(1)} %get-tuple-element.33), channel_id=1, source_target_pairs={{0,8},{8,16},{16,24},{24,0},{1,9},{9,17},{17,25},{25,1},{2,10},{10... | collective-permute-start | bytes 24584 | tf_op jit(solution)/shard_map/ppermute | solution.py:216
  111.3 5.7 %collective-permute-start.13 = (bf16[128,128]{1,0:T(8,128)(2,1)S(1)}, bf16[128,128]{1,0:T(8,128)(2,1)S(1)}, u32[]{:S(2)}, u32[]{:S(2)}) collective-permute-start(bf16[128,128]{1,0:T(8,128)(2,1)S(1)} %get-tuple-element.28), channel_id=1, source_target_pairs={{0,1},{1,0},{2,3},{3,2},{4,5},{5,4},{6,7},{7,6},{8,9},{9,8},{10,11... | collective-permute-start | bytes 98312 | tf_op jit(solution)/shard_map/ppermute | solution.py:216
  117.0 4.2 %collective-permute-start.16 = (bf16[128,128]{1,0:T(8,128)(2,1)S(1)}, bf16[128,128]{1,0:T(8,128)(2,1)S(1)}, u32[]{:S(2)}, u32[]{:S(2)}) collective-permute-start(bf16[128,128]{1,0:T(8,128)(2,1)S(1)} %add_convert_fusion.1), channel_id=1, source_target_pairs={{0,6},{2,0},{4,2},{6,4},{1,7},{3,1},{5,3},{7,5},{8,14},{10,8},{12,... | collective-permute-start | bytes 98312 | tf_op jit(solution)/shard_map/ppermute | solution.py:216
  118.4 4.0 %collective-permute-start.15 = (bf16[128,128]{1,0:T(8,128)(2,1)S(1)}, bf16[128,128]{1,0:T(8,128)(2,1)S(1)}, u32[]{:S(2)}, u32[]{:S(2)}) collective-permute-start(bf16[128,128]{1,0:T(8,128)(2,1)S(1)} %add_convert_fusion.1), channel_id=1, source_target_pairs={{0,2},{2,4},{4,6},{6,0},{1,3},{3,5},{5,7},{7,1},{8,10},{10,12},{12... | collective-permute-start | bytes 98312 | tf_op jit(solution)/shard_map/ppermute | solution.py:216
  118.5 4.3 %collective-permute-start.14 = (bf16[128,128]{1,0:T(8,128)(2,1)S(1)}, bf16[128,128]{1,0:T(8,128)(2,1)S(1)}, u32[]{:S(2)}, u32[]{:S(2)}) collective-permute-start(bf16[128,128]{1,0:T(8,128)(2,1)S(1)} %add_convert_fusion.1), channel_id=1, source_target_pairs={{0,4},{2,6},{4,0},{6,2},{1,5},{3,7},{5,1},{7,3},{8,12},{10,14},{12... | collective-permute-start | bytes 98312 | tf_op jit(solution)/shard_map/ppermute | solution.py:216
where the time goes:
time: 124 us; the launch traced here: 123 us
  waiting for transfers between devices  45 us (36%)
  starting transfers between devices  44.7 us (36%)
  blocking collectives  23.9 us (19%)
  Pallas kernels  6.31 us (5%)
  local copies, waits for them, and re-layouts  2.08 us (2%)
    ppermute x17, waiting for transfers between devices, moved(): lax.ppermute(x, axis, [(i, (i + shift) % length) for i in range(length)])  37.6 us
    ppermute x17, starting transfers between devices, moved(): lax.ppermute(x, axis, [(i, (i + shift) % length) for i in range(length)])  28.8 us
    all_to_all x1, blocking collectives, to_all(): got = lax.all_to_all(copies, axes, 0, 0, tiled=True)  12.9 us
    all_to_all x1, starting transfers between devices, shares(): return lax.all_to_all(x.reshape(-1, 8, x.shape[-1]), axes, 0, 0, tiled=True)  12 us
    all_to_all x1, blocking collectives, shares(): return lax.all_to_all(x.reshape(-1, 8, x.shape[-1]), axes, 0, 0, tiled=True)  10.9 us
    all_to_all x1, waiting for transfers between devices, to_all(): got = lax.all_to_all(copies, axes, 0, 0, tiled=True)  7.36 us
    pallas_call x5, Pallas kernels, kernel(): pl.pallas_call(whole, out_shape=tuple((pltpu.VMEM(*out) for out in outs))...  4.58 us
    all_to_all x1, starting transfers between devices, to_all(): got = lax.all_to_all(copies, axes, 0, 0, tiled=True)  3.88 us
  transfers between devices with their start and end apart: 19, of which 8 were waited for; matrix products, arithmetic and copies ran while one was open for 1% of the time, Pallas kernels for 2%

commit v1 on v0

--- a/solution.py
+++ b/solution.py
@@ -156,7 +156,9 @@
 
 
 def lift_body(mine_ref, after_ref, before_ref, across_ref, *refs):
-    sent_refs, weight_refs, (mid_ref, out_ref) = refs[:4], refs[4:8], refs[8:]
+    sent_refs, weight_refs, (gate_ref, up_ref), (mid_ref, out_ref) = refs[:4], refs[4:7], refs[7:9], refs[9:]
+    gate_from = [(ref, 0) for ref in weight_refs] + [(gate_ref, 0)]
+    up_from = [(ref, UNITS) for ref in weight_refs] + [(up_ref, 0)]
     attended = (mine_ref[...].astype(F32) + across_ref[...].astype(F32)) + (
         after_ref[...].astype(F32) + before_ref[...].astype(F32)
     )
@@ -172,15 +174,16 @@
         scaled.append((mid[:, 128 * k : 128 * k + 128] * gain).astype(BF16))
     squares = jnp.sum(mid * mid, axis=1, keepdims=True)
 
-    def product(at, size):
+    def product(weights, at, size):
         return sum(
-            dot(part, ref[at : at + size, :], ((1,), (1,))) for part, ref in zip(scaled, weight_refs)
+            dot(part, ref[base + at : base + at + size, :], ((1,), (1,)))
+            for part, (ref, base) in zip(scaled, weights)
         )
 
     for at, width in ((0, 512), (512, 512), (1024, 384)):
         real = min(width, UNITS - at)
-        low = product(at, real)
-        high = product(UNITS + at, real)
+        low = product(gate_from, at, real)
+        high = product(up_from, at, real)
         if real < width:
             pad = jnp.broadcast_to(squares, (32, width - real))
             low = jnp.concatenate([low, pad], axis=1)
@@ -232,14 +235,7 @@
     return lax.all_to_all(x.reshape(-1, 8, x.shape[-1]), axes, 0, 0, tiled=True)
 
 
-def along_y(x):
-    got = [x]
-    for k in (1, 3, 2):
-        got.append(moved(x, "y", k))
-    return tuple(got)
-
-
-def on_device(
+def layer(
     tokens,
     attn_gain,
     query_weight,
@@ -281,8 +277,8 @@
             *((a, 3 + k, 0) for k, a in enumerate(small)),
         ),
     )
-    sent = along_y(sent)
-    lifting = along_y(lifting)
+    sent = (sent, *(moved(sent, "y", k) for k in (1, 3, 2)))
+    before, after = (moved(lifting, "y", k) for k in (1, 3))
     caches = (decay_cache[:, :, 0], key_cache[:, :, 0], value_cache[:, :, 0], carried_state[:, 0])
     heads, new_keys, new_values = pl.pallas_call(
         attend_body,
@@ -297,8 +293,11 @@
         name="attend",
     )(shares(first, KV), *small, *map(in_hbm, caches))
     (attended,) = kernel(out_body, [((32, 512), BF16)], (to_all(heads, "z"), *sent))
+    across = (moved(before[:UNITS], "y", 1), moved(after[UNITS:], "y", 3))
     middle, second = kernel(
-        lift_body, [((4, 32, 128), BF16), ((4, 2, 8, SECOND), BF16)], (*tp_parts(attended), *sent, *lifting)
+        lift_body,
+        [((4, 32, 128), BF16), ((4, 2, 8, SECOND), BF16)],
+        (*tp_parts(attended), *sent, lifting, before, after, *across),
     )
     (hidden,) = kernel(hidden_body, [((seqs, SECOND), BF16)], (shares(second, "z"),))
     middles = (middle[0], moved(middle[2], "y", 1), moved(middle[1], "y", 3), moved(middle[3], "y", 2))
@@ -335,6 +334,4 @@
         P(TP, KV),
     )
     out_specs = (P(None, KV), P(KV, TP, None), P(KV, TP, None))
-    return jax.shard_map(
-        on_device, mesh=axes, in_specs=in_specs, out_specs=out_specs, check_vma=False
-    )
+    return jax.shard_map(layer, mesh=axes, in_specs=in_specs, out_specs=out_specs, check_vma=False)

time: 124 us -> 103 us (0.83)
  waiting for transfers between devices: 45 us -> 16.1 us
  starting transfers between devices: 44.7 us -> 49.2 us
  blocking collectives: 23.9 us -> 26.1 us
  local copies, waits for them, and re-layouts: 2.08 us -> 3.58 us
    ppermute x17 -> x18, waiting for transfers between devices: 37.6 us -> 9.2 us  [moved(): lax.ppermute(x, axis, [(i, (i + shift) % length) for i in range(length)])]
    ppermute x17 -> x18, starting transfers between devices: 28.8 us -> 33.4 us  [moved(): lax.ppermute(x, axis, [(i, (i + shift) % length) for i in range(length)])]
    all_to_all x1, blocking collectives: 12.9 us -> 15.2 us  [to_all(): got = lax.all_to_all(copies, axes, 0, 0, tiled=True)]
    slice x0 -> x2, local copies, waits for them, and re-layouts: none -> 1.51 us  [layer(): across = (moved(before[:UNITS], 'y', 1), moved(after[UNITS:], 'y', 3))]
  transfers between devices with their start and end apart: 19 -> 20, of which waited for: 8 -> 9; matrix products, arithmetic and copies ran while one was open for 1% -> 3% of each run, Pallas kernels for 2% -> 2%
where the time goes in v1:
time: 103 us
  starting transfers between devices  49.2 us (48%)
  blocking collectives  26.1 us (25%)
  waiting for transfers between devices  16.1 us (16%)
  Pallas kernels  6.31 us (6%)
  local copies, waits for them, and re-layouts  3.58 us (3%)
    ppermute x18, starting transfers between devices, moved(): lax.ppermute(x, axis, [(i, (i + shift) % length) for i in range(length)])  33.4 us
    all_to_all x1, blocking collectives, to_all(): got = lax.all_to_all(copies, axes, 0, 0, tiled=True)  15.2 us
    all_to_all x1, starting transfers between devices, shares(): return lax.all_to_all(x.reshape(-1, 8, x.shape[-1]), axes, 0, 0, tiled=True)  11 us
    all_to_all x1, blocking collectives, shares(): return lax.all_to_all(x.reshape(-1, 8, x.shape[-1]), axes, 0, 0, tiled=True)  10.9 us
    ppermute x18, waiting for transfers between devices, moved(): lax.ppermute(x, axis, [(i, (i + shift) % length) for i in range(length)])  9.2 us
    all_to_all x1, waiting for transfers between devices, to_all(): got = lax.all_to_all(copies, axes, 0, 0, tiled=True)  6.88 us
    all_to_all x1, starting transfers between devices, to_all(): got = lax.all_to_all(copies, axes, 0, 0, tiled=True)  4.88 us
    pallas_call x5, Pallas kernels, kernel(): pl.pallas_call(whole, out_shape=tuple((pltpu.VMEM(*out) for out in outs))...  4.58 us
  transfers between devices with their start and end apart: 20, of which 9 were waited for; matrix products, arithmetic and copies ran while one was open for 3% of the time, Pallas kernels for 2%

profile of v1, /device:TPU:1, one launch (start us, length us, event | category | flops | bytes accessed | tf_op | source)
XLA Modules:
  0.0 102.8 jit_solution(9285523854496811296)
XLA Ops:
  0.6 2.9 %shard_map.211 = (bf16[16,2,8,512]{3,2,1,0:T(8,128)(2,1)}, bf16[400,128]{1,0:T(8,128)(2,1)S(1)}, bf16[2752,128]{1,0:T(8,128)(2,1)S(1)}, bf16[16,128]{1,0:T(8,128...) custom-call(bf16[128,128]{1,0:T(8,128)(2,1)} %refs_9_.1, f32[1,128]{1,0:T(1,128)} %bitcast.35, ...), custom_call_target="tpu_custom_call" | custom-call | tf_op jit(solution)/shard_map/pallas_call | solution.py:44
  3.5 3.6 %collective-permute-start.8 = (bf16[2752,128]{1,0:T(8,128)(2,1)S(1)}, bf16[2752,128]{1,0:T(8,128)(2,1)S(1)}, u32[]{:S(2)}, u32[]{:S(2)}) collective-permute-start(bf16[2752,128]{1,0:T(8,128)(2,1)S(1)} %get-tuple-element.24.refs_8_), channel_id=1, source_target_pairs={{0,24},{8,0},{16,8},{24,16},{1,25},{9,1},{17,9},{25,17},{2,26},{10... | collective-permute-start | bytes 2113544 | tf_op jit(solution)/shard_map/ppermute | solution.py:219
  7.2 11.0 %all-to-all-start = ((bf16[32,8,512]{2,1,0:T(8,128)(2,1)}), bf16[32,8,512]{2,1,0:T(8,128)(2,1)S(1)}, u32[]{:S(2)}, u32[]{:S(2)}) async-start(bf16[32,8,512]{2,1,0:T(8,128)(2,1)} %bitcast.8), calls=%async_computation | async-start | bytes 524288 | tf_op jit(solution)/shard_map/all_to_all | solution.py:235
  18.1 2.8 %collective-permute-start.2 = (bf16[400,128]{1,0:T(8,128)(2,1)S(1)}, bf16[400,128]{1,0:T(8,128)(2,1)S(1)}, u32[]{:S(2)}, u32[]{:S(2)}) collective-permute-start(bf16[400,128]{1,0:T(8,128)(2,1)S(1)} %get-tuple-element.23.refs_1_.refs_4_), channel_id=1, source_target_pairs={{0,16},{8,24},{16,0},{24,8},{1,17},{9,25},{17,1},{25,9},{2,18},{10... | collective-permute-start | bytes 307208 | tf_op jit(solution)/shard_map/ppermute | solution.py:219
  21.0 0.9 collective-permute-start.1
  22.4 1.3 %collective-permute-done.8.refs_10_ = bf16[2752,128]{1,0:T(8,128)(2,1)S(1)} collective-permute-done((bf16[2752,128]{1,0:T(8,128)(2,1)S(1)}, bf16[2752,128]{1,0:T(8,128)(2,1)S(1)}, u32[]{:S(2)}, u32[]{:S(2)}) %collective-permute-start.8) | collective-permute-done | bytes 704544 | tf_op jit(solution)/shard_map/ppermute | solution.py:219
  23.7 0.8 slice.25
  24.5 4.6 %collective-permute-start.10 = (bf16[1376,128]{1,0:T(8,128)(2,1)}, bf16[1376,128]{1,0:T(8,128)(2,1)S(1)}, u32[]{:S(2)}, u32[]{:S(2)}) collective-permute-start(bf16[1376,128]{1,0:T(8,128)(2,1)} %slice.25), channel_id=1, source_target_pairs={{0,24},{8,0},{16,8},{24,16},{1,25},{9,1},{17,9},{25,17},{2,26},{10... | collective-permute-start | bytes 1056776 | tf_op jit(solution)/shard_map/ppermute | solution.py:219
  29.1 0.8 slice.24
  29.9 1.7 %attend.1 = (bf16[4,256]{1,0:T(4,128)(2,1)S(1)}, bf16[4,128]{1,0:T(4,128)(2,1)S(1)}, bf16[4,256]{1,0:T(4,128)(2,1)S(1)}) custom-call(bf16[32,8,512]{2,1,0:T(8,128)(2,1)S(1)} %all-to-all-done.got_ref, bf16[16,128]{1,0:T(8,128)(2,1)S(1)} %get-tuple-element.18.dw_ref, f32[1,128]{1,0:T(1,128)S(1)} %get-tuple-element.19.bias_ref, ...), custom_call_target="tpu_custom_call" | custom-call | tf_op jit(solution)/shard_map/attend/pallas_call | solution.py:283
  31.7 15.2 %all_to_all.20 = bf16[8,4,256]{2,1,0:T(4,128)(2,1)S(1)} all-to-all(bf16[8,4,256]{2,1,0:T(4,128)(2,1)S(1)} %broadcast_in_dim.38), channel_id=1, replica_groups=mesh['z'=8,'y'=4,'x'=4,'c'=2] {'z'}, dimensions={0} | all-to-all | bytes 32768 | tf_op jit(solution)/shard_map/all_to_all | solution.py:230
  47.1 5.4 %collective-permute-start.3 = (bf16[32,512]{1,0:T(8,128)(2,1)S(1)}, bf16[32,512]{1,0:T(8,128)(2,1)S(1)}, u32[]{:S(2)}, u32[]{:S(2)}) collective-permute-start(bf16[32,512]{1,0:T(8,128)(2,1)S(1)} %shard_map.212), channel_id=1, source_target_pairs={{0,1},{1,0},{2,3},{3,2},{4,5},{5,4},{6,7},{7,6},{8,9},{9,8},{10,11... | collective-permute-start | bytes 98312 | tf_op jit(solution)/shard_map/ppermute | solution.py:219
  52.4 0.9 collective-permute-done.3
  53.3 2.8 %collective-permute-start.6 = (bf16[32,512]{1,0:T(8,128)(2,1)S(1)}, bf16[32,512]{1,0:T(8,128)(2,1)S(1)}, u32[]{:S(2)}, u32[]{:S(2)}) collective-permute-start(bf16[32,512]{1,0:T(8,128)(2,1)S(1)} %add_convert_fusion.2.refs_0_), channel_id=1, source_target_pairs={{0,4},{2,6},{4,0},{6,2},{1,5},{3,7},{5,1},{7,3},{8,12},{10,14},{12... | collective-permute-start | bytes 98312 | tf_op jit(solution)/shard_map/ppermute | solution.py:219
  56.1 0.9 collective-permute-start.5
  57.0 0.6 collective-permute-start.4
  57.7 1.2 %collective-permute-done.5.refs_2_ = bf16[32,512]{1,0:T(8,128)(2,1)S(1)} collective-permute-done((bf16[32,512]{1,0:T(8,128)(2,1)S(1)}, bf16[32,512]{1,0:T(8,128)(2,1)S(1)}, u32[]{:S(2)}, u32[]{:S(2)}) %collective-permute-start.5) | collective-permute-done | bytes 32800 | tf_op jit(solution)/shard_map/ppermute | solution.py:219
  58.9 2.1 %collective-permute-done.4.refs_1_ = bf16[32,512]{1,0:T(8,128)(2,1)S(1)} collective-permute-done((bf16[32,512]{1,0:T(8,128)(2,1)S(1)}, bf16[32,512]{1,0:T(8,128)(2,1)S(1)}, u32[]{:S(2)}, u32[]{:S(2)}) %collective-permute-start.4) | collective-permute-done | bytes 32800 | tf_op jit(solution)/shard_map/ppermute | solution.py:219
  61.0 1.2 %shard_map.213 = (bf16[4,32,128]{2,1,0:T(8,128)(2,1)S(1)}, bf16[4,2,8,1408]{3,2,1,0:T(8,128)(2,1)S(1)}) custom-call(bf16[32,512]{1,0:T(8,128)(2,1)S(1)} %add_convert_fusion.2.refs_0_, bf16[32,512]{1,0:T(8,128)(2,1)S(1)} %collective-permute-done.4.refs_1_, bf16[32,512]{1,0:T(8,128)(2,1)S(1)} %collective-permute-done.5.refs_2_, ...), custom_call_target="tpu_custom_call" | custom-call | tf_op jit(solution)/shard_map/pallas_call | solution.py:44
  62.1 10.9 %all_to_all.21.refs_0_ = bf16[8,8,1408]{2,1,0:T(8,128)(2,1)S(1)} all-to-all(bf16[8,8,1408]{2,1,0:T(8,128)(2,1)S(1)} %bitcast.26), channel_id=1, replica_groups=mesh['z'=8,'y'=4,'x'=4,'c'=2] {'z'}, dimensions={0} | all-to-all | bytes 360448 | tf_op jit(solution)/shard_map/all_to_all | solution.py:235
  73.1 0.8 broadcast_in_dim.39
  74.0 4.9 %all-to-all-start.3 = ((bf16[32,4,1408]{2,1,0:T(4,128)(2,1)}), bf16[32,4,1408]{2,1,0:T(4,128)(2,1)S(1)}, u32[]{:S(2)}, u32[]{:S(2)}) async-start(bf16[32,4,1408]{2,1,0:T(4,128)(2,1)} %broadcast_in_dim.39), calls=%async_computation.3 | async-start | bytes 720896 | tf_op jit(solution)/shard_map/all_to_all | solution.py:230
  78.9 2.8 %collective-permute-start.13 = (bf16[32,128]{1,0:T(8,128)(2,1)S(1)}, bf16[32,128]{1,0:T(8,128)(2,1)S(1)}, u32[]{:S(2)}, u32[]{:S(2)}) collective-permute-start(bf16[32,128]{1,0:T(8,128)(2,1)S(1)} %get-tuple-element.31), channel_id=1, source_target_pairs={{0,16},{8,24},{16,0},{24,8},{1,17},{9,25},{17,1},{25,9},{2,18},{10... | collective-permute-start | bytes 24584 | tf_op jit(solution)/shard_map/ppermute | solution.py:219
  81.7 0.9 collective-permute-start.12
  83.2 6.9 %all-to-all-done.3 = bf16[32,4,1408]{2,1,0:T(4,128)(2,1)S(1)} async-done(((bf16[32,4,1408]{2,1,0:T(4,128)(2,1)}), bf16[32,4,1408]{2,1,0:T(4,128)(2,1)S(1)}, u32[]{:S(2)}, u32[]{:S(2)}) %all-to-all-start.3) | async-done | bytes 360480 | tf_op jit(solution)/shard_map/all_to_all | solution.py:230
  90.4 4.9 %collective-permute-start.14 = (bf16[128,128]{1,0:T(8,128)(2,1)S(1)}, bf16[128,128]{1,0:T(8,128)(2,1)S(1)}, u32[]{:S(2)}, u32[]{:S(2)}) collective-permute-start(bf16[128,128]{1,0:T(8,128)(2,1)S(1)} %get-tuple-element.28), channel_id=1, source_target_pairs={{0,1},{1,0},{2,3},{3,2},{4,5},{5,4},{6,7},{7,6},{8,9},{9,8},{10,11... | collective-permute-start | bytes 98312 | tf_op jit(solution)/shard_map/ppermute | solution.py:219
  95.3 0.9 collective-permute-done.14
  96.2 0.6 collective-permute-start.17
  96.8 0.9 collective-permute-start.16
  99.3 1.5 %collective-permute-done.16 = bf16[128,128]{1,0:T(8,128)(2,1)S(1)} collective-permute-done((bf16[128,128]{1,0:T(8,128)(2,1)S(1)}, bf16[128,128]{1,0:T(8,128)(2,1)S(1)}, u32[]{:S(2)}, u32[]{:S(2)}) %collective-permute-start.16) | collective-permute-done | bytes 32800 | tf_op jit(solution)/shard_map/ppermute | solution.py:219
  100.8 1.3 %collective-permute-done.15 = bf16[128,128]{1,0:T(8,128)(2,1)S(1)} collective-permute-done((bf16[128,128]{1,0:T(8,128)(2,1)S(1)}, bf16[128,128]{1,0:T(8,128)(2,1)S(1)}, u32[]{:S(2)}, u32[]{:S(2)}) %collective-permute-start.15) | collective-permute-done | bytes 32800 | tf_op jit(solution)/shard_map/ppermute | solution.py:219
  102.1 0.6 add_convert_fusion
  (30 shorter events, 3.5 us)
Async XLA Ops:
  3.5 20.2 %collective-permute-start.8 = (bf16[2752,128]{1,0:T(8,128)(2,1)S(1)}, bf16[2752,128]{1,0:T(8,128)(2,1)S(1)}, u32[]{:S(2)}, u32[]{:S(2)}) collective-permute-start(bf16[2752,128]{1,0:T(8,128)(2,1)S(1)} %get-tuple-element.24.refs_8_), channel_id=1, source_target_pairs={{0,24},{8,0},{16,8},{24,16},{1,25},{9,1},{17,9},{25,17},{2,26},{10... | collective-permute-start | bytes 2113544 | tf_op jit(solution)/shard_map/ppermute | solution.py:219
  7.2 22.0 %collective-permute-start.7 = (bf16[2752,128]{1,0:T(8,128)(2,1)S(1)}, bf16[2752,128]{1,0:T(8,128)(2,1)S(1)}, u32[]{:S(2)}, u32[]{:S(2)}) collective-permute-start(bf16[2752,128]{1,0:T(8,128)(2,1)S(1)} %get-tuple-element.24.refs_8_), channel_id=1, source_target_pairs={{0,8},{8,16},{16,24},{24,0},{1,9},{9,17},{17,25},{25,1},{2,10},{10... | collective-permute-start | bytes 2113544 | tf_op jit(solution)/shard_map/ppermute | solution.py:219
  7.2 22.7 %all-to-all-start = ((bf16[32,8,512]{2,1,0:T(8,128)(2,1)}), bf16[32,8,512]{2,1,0:T(8,128)(2,1)S(1)}, u32[]{:S(2)}, u32[]{:S(2)}) async-start(bf16[32,8,512]{2,1,0:T(8,128)(2,1)} %bitcast.8), calls=%async_computation | async-start | bytes 524288 | tf_op jit(solution)/shard_map/all_to_all | solution.py:235
  18.1 28.7 %collective-permute-start.2 = (bf16[400,128]{1,0:T(8,128)(2,1)S(1)}, bf16[400,128]{1,0:T(8,128)(2,1)S(1)}, u32[]{:S(2)}, u32[]{:S(2)}) collective-permute-start(bf16[400,128]{1,0:T(8,128)(2,1)S(1)} %get-tuple-element.23.refs_1_.refs_4_), channel_id=1, source_target_pairs={{0,16},{8,24},{16,0},{24,8},{1,17},{9,25},{17,1},{25,9},{2,18},{10... | collective-permute-start | bytes 307208 | tf_op jit(solution)/shard_map/ppermute | solution.py:219
  21.0 25.9 %collective-permute-start.1 = (bf16[400,128]{1,0:T(8,128)(2,1)S(1)}, bf16[400,128]{1,0:T(8,128)(2,1)S(1)}, u32[]{:S(2)}, u32[]{:S(2)}) collective-permute-start(bf16[400,128]{1,0:T(8,128)(2,1)S(1)} %get-tuple-element.23.refs_1_.refs_4_), channel_id=1, source_target_pairs={{0,24},{8,0},{16,8},{24,16},{1,25},{9,1},{17,9},{25,17},{2,26},{10... | collective-permute-start | bytes 307208 | tf_op jit(solution)/shard_map/ppermute | solution.py:219
  21.9 25.0 %collective-permute-start = (bf16[400,128]{1,0:T(8,128)(2,1)S(1)}, bf16[400,128]{1,0:T(8,128)(2,1)S(1)}, u32[]{:S(2)}, u32[]{:S(2)}) collective-permute-start(bf16[400,128]{1,0:T(8,128)(2,1)S(1)} %get-tuple-element.23.refs_1_.refs_4_), channel_id=1, source_target_pairs={{0,8},{8,16},{16,24},{24,0},{1,9},{9,17},{17,25},{25,1},{2,10},{10... | collective-permute-start | bytes 307208 | tf_op jit(solution)/shard_map/ppermute | solution.py:219
  24.5 36.5 %collective-permute-start.10 = (bf16[1376,128]{1,0:T(8,128)(2,1)}, bf16[1376,128]{1,0:T(8,128)(2,1)S(1)}, u32[]{:S(2)}, u32[]{:S(2)}) collective-permute-start(bf16[1376,128]{1,0:T(8,128)(2,1)} %slice.25), channel_id=1, source_target_pairs={{0,24},{8,0},{16,8},{24,16},{1,25},{9,1},{17,9},{25,17},{2,26},{10... | collective-permute-start | bytes 1056776 | tf_op jit(solution)/shard_map/ppermute | solution.py:219
  29.9 31.1 %collective-permute-start.9 = (bf16[1376,128]{1,0:T(8,128)(2,1)}, bf16[1376,128]{1,0:T(8,128)(2,1)S(1)}, u32[]{:S(2)}, u32[]{:S(2)}) collective-permute-start(bf16[1376,128]{1,0:T(8,128)(2,1)} %slice.24), channel_id=1, source_target_pairs={{0,8},{8,16},{16,24},{24,0},{1,9},{9,17},{17,25},{25,1},{2,10},{10... | collective-permute-start | bytes 1056776 | tf_op jit(solution)/shard_map/ppermute | solution.py:219
  47.1 6.2 %collective-permute-start.3 = (bf16[32,512]{1,0:T(8,128)(2,1)S(1)}, bf16[32,512]{1,0:T(8,128)(2,1)S(1)}, u32[]{:S(2)}, u32[]{:S(2)}) collective-permute-start(bf16[32,512]{1,0:T(8,128)(2,1)S(1)} %shard_map.212), channel_id=1, source_target_pairs={{0,1},{1,0},{2,3},{3,2},{4,5},{5,4},{6,7},{7,6},{8,9},{9,8},{10,11... | collective-permute-start | bytes 98312 | tf_op jit(solution)/shard_map/ppermute | solution.py:219
  53.3 4.4 %collective-permute-start.6 = (bf16[32,512]{1,0:T(8,128)(2,1)S(1)}, bf16[32,512]{1,0:T(8,128)(2,1)S(1)}, u32[]{:S(2)}, u32[]{:S(2)}) collective-permute-start(bf16[32,512]{1,0:T(8,128)(2,1)S(1)} %add_convert_fusion.2.refs_0_), channel_id=1, source_target_pairs={{0,4},{2,6},{4,0},{6,2},{1,5},{3,7},{5,1},{7,3},{8,12},{10,14},{12... | collective-permute-start | bytes 98312 | tf_op jit(solution)/shard_map/ppermute | solution.py:219
  56.1 2.8 %collective-permute-start.5 = (bf16[32,512]{1,0:T(8,128)(2,1)S(1)}, bf16[32,512]{1,0:T(8,128)(2,1)S(1)}, u32[]{:S(2)}, u32[]{:S(2)}) collective-permute-start(bf16[32,512]{1,0:T(8,128)(2,1)S(1)} %add_convert_fusion.2.refs_0_), channel_id=1, source_target_pairs={{0,6},{2,0},{4,2},{6,4},{1,7},{3,1},{5,3},{7,5},{8,14},{10,8},{12,... | collective-permute-start | bytes 98312 | tf_op jit(solution)/shard_map/ppermute | solution.py:219
  57.0 4.0 %collective-permute-start.4 = (bf16[32,512]{1,0:T(8,128)(2,1)S(1)}, bf16[32,512]{1,0:T(8,128)(2,1)S(1)}, u32[]{:S(2)}, u32[]{:S(2)}) collective-permute-start(bf16[32,512]{1,0:T(8,128)(2,1)S(1)} %add_convert_fusion.2.refs_0_), channel_id=1, source_target_pairs={{0,2},{2,4},{4,6},{6,0},{1,3},{3,5},{5,7},{7,1},{8,10},{10,12},{12... | collective-permute-start | bytes 98312 | tf_op jit(solution)/shard_map/ppermute | solution.py:219
  74.0 16.1 %all-to-all-start.3 = ((bf16[32,4,1408]{2,1,0:T(4,128)(2,1)}), bf16[32,4,1408]{2,1,0:T(4,128)(2,1)S(1)}, u32[]{:S(2)}, u32[]{:S(2)}) async-start(bf16[32,4,1408]{2,1,0:T(4,128)(2,1)} %broadcast_in_dim.39), calls=%async_computation.3 | async-start | bytes 720896 | tf_op jit(solution)/shard_map/all_to_all | solution.py:230
  78.9 11.3 %collective-permute-start.13 = (bf16[32,128]{1,0:T(8,128)(2,1)S(1)}, bf16[32,128]{1,0:T(8,128)(2,1)S(1)}, u32[]{:S(2)}, u32[]{:S(2)}) collective-permute-start(bf16[32,128]{1,0:T(8,128)(2,1)S(1)} %get-tuple-element.31), channel_id=1, source_target_pairs={{0,16},{8,24},{16,0},{24,8},{1,17},{9,25},{17,1},{25,9},{2,18},{10... | collective-permute-start | bytes 24584 | tf_op jit(solution)/shard_map/ppermute | solution.py:219
  81.7 8.5 %collective-permute-start.12 = (bf16[32,128]{1,0:T(8,128)(2,1)S(1)}, bf16[32,128]{1,0:T(8,128)(2,1)S(1)}, u32[]{:S(2)}, u32[]{:S(2)}) collective-permute-start(bf16[32,128]{1,0:T(8,128)(2,1)S(1)} %get-tuple-element.32), channel_id=1, source_target_pairs={{0,24},{8,0},{16,8},{24,16},{1,25},{9,1},{17,9},{25,17},{2,26},{10... | collective-permute-start | bytes 24584 | tf_op jit(solution)/shard_map/ppermute | solution.py:219
  82.6 7.6 %copy-start = (bf16[1376,128]{1,0:T(8,128)(2,1)S(1)}, bf16[1376,128]{1,0:T(8,128)(2,1)}, u32[]{:S(2)}) copy-start(bf16[1376,128]{1,0:T(8,128)(2,1)} %refs_1_.1) | copy-start | bytes 1056772
  82.6 7.6 %collective-permute-start.11 = (bf16[32,128]{1,0:T(8,128)(2,1)S(1)}, bf16[32,128]{1,0:T(8,128)(2,1)S(1)}, u32[]{:S(2)}, u32[]{:S(2)}) collective-permute-start(bf16[32,128]{1,0:T(8,128)(2,1)S(1)} %get-tuple-element.33), channel_id=1, source_target_pairs={{0,8},{8,16},{16,24},{24,0},{1,9},{9,17},{17,25},{25,1},{2,10},{10... | collective-permute-start | bytes 24584 | tf_op jit(solution)/shard_map/ppermute | solution.py:219
  90.4 5.8 %collective-permute-start.14 = (bf16[128,128]{1,0:T(8,128)(2,1)S(1)}, bf16[128,128]{1,0:T(8,128)(2,1)S(1)}, u32[]{:S(2)}, u32[]{:S(2)}) collective-permute-start(bf16[128,128]{1,0:T(8,128)(2,1)S(1)} %get-tuple-element.28), channel_id=1, source_target_pairs={{0,1},{1,0},{2,3},{3,2},{4,5},{5,4},{6,7},{7,6},{8,9},{9,8},{10,11... | collective-permute-start | bytes 98312 | tf_op jit(solution)/shard_map/ppermute | solution.py:219
  96.2 3.1 %collective-permute-start.17 = (bf16[128,128]{1,0:T(8,128)(2,1)S(1)}, bf16[128,128]{1,0:T(8,128)(2,1)S(1)}, u32[]{:S(2)}, u32[]{:S(2)}) collective-permute-start(bf16[128,128]{1,0:T(8,128)(2,1)S(1)} %add_convert_fusion.1), channel_id=1, source_target_pairs={{0,6},{2,0},{4,2},{6,4},{1,7},{3,1},{5,3},{7,5},{8,14},{10,8},{12,... | collective-permute-start | bytes 98312 | tf_op jit(solution)/shard_map/ppermute | solution.py:219
  96.8 4.0 %collective-permute-start.16 = (bf16[128,128]{1,0:T(8,128)(2,1)S(1)}, bf16[128,128]{1,0:T(8,128)(2,1)S(1)}, u32[]{:S(2)}, u32[]{:S(2)}) collective-permute-start(bf16[128,128]{1,0:T(8,128)(2,1)S(1)} %add_convert_fusion.1), channel_id=1, source_target_pairs={{0,2},{2,4},{4,6},{6,0},{1,3},{3,5},{5,7},{7,1},{8,10},{10,12},{12... | collective-permute-start | bytes 98312 | tf_op jit(solution)/shard_map/ppermute | solution.py:219
  97.8 4.4 %collective-permute-start.15 = (bf16[128,128]{1,0:T(8,128)(2,1)S(1)}, bf16[128,128]{1,0:T(8,128)(2,1)S(1)}, u32[]{:S(2)}, u32[]{:S(2)}) collective-permute-start(bf16[128,128]{1,0:T(8,128)(2,1)S(1)} %add_convert_fusion.1), channel_id=1, source_target_pairs={{0,4},{2,6},{4,0},{6,2},{1,5},{3,7},{5,1},{7,3},{8,12},{10,14},{12... | collective-permute-start | bytes 98312 | tf_op jit(solution)/shard_map/ppermute | solution.py:219

commit v2 on v1

--- a/solution.py
+++ b/solution.py
@@ -156,9 +156,7 @@
 
 
 def lift_body(mine_ref, after_ref, before_ref, across_ref, *refs):
-    sent_refs, weight_refs, (gate_ref, up_ref), (mid_ref, out_ref) = refs[:4], refs[4:7], refs[7:9], refs[9:]
-    gate_from = [(ref, 0) for ref in weight_refs] + [(gate_ref, 0)]
-    up_from = [(ref, UNITS) for ref in weight_refs] + [(up_ref, 0)]
+    sent_refs, gate_refs, up_refs, (mid_ref, out_ref) = refs[:4], refs[4:8], refs[8:12], refs[12:]
     attended = (mine_ref[...].astype(F32) + across_ref[...].astype(F32)) + (
         after_ref[...].astype(F32) + before_ref[...].astype(F32)
     )
@@ -176,14 +174,13 @@
 
     def product(weights, at, size):
         return sum(
-            dot(part, ref[base + at : base + at + size, :], ((1,), (1,)))
-            for part, (ref, base) in zip(scaled, weights)
+            dot(part, ref[at : at + size, :], ((1,), (1,))) for part, ref in zip(scaled, weights)
         )
 
     for at, width in ((0, 512), (512, 512), (1024, 384)):
         real = min(width, UNITS - at)
-        low = product(gate_from, at, real)
-        high = product(up_from, at, real)
+        low = product(gate_refs, at, real)
+        high = product(up_refs, at, real)
         if real < width:
             pad = jnp.broadcast_to(squares, (32, width - real))
             low = jnp.concatenate([low, pad], axis=1)
@@ -260,26 +257,26 @@
     seqs = key_cache.shape[0]
     read = (tokens, attn_gain[None], query_weight, key_weight, value_weight, outgate_weight, code_weight.T)
     small = (decay_weight, decay_bias[None], head_gain[None], lengths[None])
-    first, sent, lifting, *small = kernel(
+    gate, up = gate_weight.T, up_weight.T
+    first, sent, *small = kernel(
         project_body,
         [
             ((32 // 2, 2, 8, FIRST), BF16),
             ((SENT, 128), BF16),
-            ((2 * UNITS, 128), BF16),
             *((a.shape, a.dtype) for a in small),
         ],
         [in_hbm(a) for a in (*read, mlp_gain[None])],
         (
             (output_weight, 1, 0),
             (tokens, 1, TOKENS_AT),
-            (gate_weight.T, 2, 0),
-            (up_weight.T, 2, UNITS),
-            *((a, 3 + k, 0) for k, a in enumerate(small)),
+            *((a, 2 + k, 0) for k, a in enumerate(small)),
         ),
     )
     sent = (sent, *(moved(sent, "y", k) for k in (1, 3, 2)))
-    before, after = (moved(lifting, "y", k) for k in (1, 3))
+    gates = [gate, *(moved(gate, "y", k) for k in (1, 3))]
+    ups = [up, *(moved(up, "y", k) for k in (1, 3))]
     caches = (decay_cache[:, :, 0], key_cache[:, :, 0], value_cache[:, :, 0], carried_state[:, 0])
+    first = shares(first, KV)
     heads, new_keys, new_values = pl.pallas_call(
         attend_body,
         out_shape=(pltpu.VMEM((seqs, 256), BF16), pltpu.VMEM((seqs, 128), BF16), pltpu.VMEM((seqs, 256), BF16)),
@@ -291,13 +288,13 @@
         ],
         compiler_params=pltpu.CompilerParams(vmem_limit_bytes=8 << 20),
         name="attend",
-    )(shares(first, KV), *small, *map(in_hbm, caches))
-    (attended,) = kernel(out_body, [((32, 512), BF16)], (to_all(heads, "z"), *sent))
-    across = (moved(before[:UNITS], "y", 1), moved(after[UNITS:], "y", 3))
+    )(first, *small, *map(in_hbm, caches))
+    heads = to_all(heads, "z")
+    (attended,) = kernel(out_body, [((32, 512), BF16)], (heads, *sent))
+    gates.append(moved(gates[1], "y", 1))
+    ups.append(moved(ups[2], "y", 3))
     middle, second = kernel(
-        lift_body,
-        [((4, 32, 128), BF16), ((4, 2, 8, SECOND), BF16)],
-        (*tp_parts(attended), *sent, lifting, before, after, *across),
+        lift_body, [((4, 32, 128), BF16), ((4, 2, 8, SECOND), BF16)], (*tp_parts(attended), *sent, *gates, *ups)
     )
     (hidden,) = kernel(hidden_body, [((seqs, SECOND), BF16)], (shares(second, "z"),))
     middles = (middle[0], moved(middle[2], "y", 1), moved(middle[1], "y", 3), moved(middle[3], "y", 2))

time: 103 us -> 105 us (1.019)
  waiting for transfers between devices: 16.1 us -> 25 us
  starting transfers between devices: 49.2 us -> 44.8 us
  local copies, waits for them, and re-layouts: 3.58 us -> 2.1 us
  blocking collectives: 26.1 us -> 24.8 us
    ppermute x18 -> x20, waiting for transfers between devices: 9.2 us -> 17.9 us  [moved(): lax.ppermute(x, axis, [(i, (i + shift) % length) for i in range(length)])]
    ppermute x18 -> x20, starting transfers between devices: 33.4 us -> 28.9 us  [moved(): lax.ppermute(x, axis, [(i, (i + shift) % length) for i in range(length)])]
    slice x2 -> x0, local copies, waits for them, and re-layouts: 1.51 us -> none  [layer(): across = (moved(before[:UNITS], 'y', 1), moved(after[UNITS:], 'y', 3))]
    all_to_all x1, blocking collectives: 15.2 us -> 13.9 us  [to_all(): got = lax.all_to_all(copies, axes, 0, 0, tiled=True)]
    all_to_all x1, starting transfers between devices: 11 us -> 12 us  [shares(): return lax.all_to_all(x.reshape(-1, 8, x.shape[-1]), axes, 0, 0, tiled=True)]
  transfers between devices with their start and end apart: 20 -> 22, of which waited for: 9 -> 10; matrix products, arithmetic and copies ran while one was open for 3% -> 1% of each run, Pallas kernels for 2% -> 2%
where the time goes in v2:
time: 105 us; the launch traced here: 104 us
  starting transfers between devices  44.8 us (43%)
  waiting for transfers between devices  25 us (24%)
  blocking collectives  24.8 us (24%)
  Pallas kernels  6 us (6%)
  local copies, waits for them, and re-layouts  2.1 us (2%)
    ppermute x20, starting transfers between devices, moved(): lax.ppermute(x, axis, [(i, (i + shift) % length) for i in range(length)])  28.9 us
    ppermute x20, waiting for transfers between devices, moved(): lax.ppermute(x, axis, [(i, (i + shift) % length) for i in range(length)])  17.9 us
    all_to_all x1, blocking collectives, to_all(): got = lax.all_to_all(copies, axes, 0, 0, tiled=True)  13.9 us
    all_to_all x1, starting transfers between devices, shares(): return lax.all_to_all(x.reshape(-1, 8, x.shape[-1]), axes, 0, 0, tiled=True)  12 us
    all_to_all x1, blocking collectives, shares(): return lax.all_to_all(x.reshape(-1, 8, x.shape[-1]), axes, 0, 0, tiled=True)  10.9 us
    all_to_all x1, waiting for transfers between devices, to_all(): got = lax.all_to_all(copies, axes, 0, 0, tiled=True)  7.09 us
    pallas_call x5, Pallas kernels, kernel(): pl.pallas_call(whole, out_shape=tuple((pltpu.VMEM(*out) for out in outs))...  4.27 us
    all_to_all x1, starting transfers between devices, to_all(): got = lax.all_to_all(copies, axes, 0, 0, tiled=True)  3.87 us
  transfers between devices with their start and end apart: 22, of which 10 were waited for; matrix products, arithmetic and copies ran while one was open for 1% of the time, Pallas kernels for 2%

profile of v2, /device:TPU:1, one launch (start us, length us, event | category | flops | bytes accessed | tf_op | source)
XLA Modules:
  0.0 104.2 jit_solution(15921323983911081709)
XLA Ops:
  0.7 2.6 %shard_map.211 = (bf16[16,2,8,512]{3,2,1,0:T(8,128)(2,1)}, bf16[400,128]{1,0:T(8,128)(2,1)S(1)}, bf16[16,128]{1,0:T(8,128)(2,1)S(1)}, f32[1,128]{1,0:T(1,128)S(1...) custom-call(bf16[128,128]{1,0:T(8,128)(2,1)} %refs_9_.1, f32[1,128]{1,0:T(1,128)} %bitcast.39, bf16[128,128]{1,0:T(8,128)(2,1)} %refs_2_.1, ...), custom_call_target="tpu_custom_call" | custom-call | tf_op jit(solution)/shard_map/pallas_call | solution.py:44
  3.2 12.0 %all-to-all-start = ((bf16[32,8,512]{2,1,0:T(8,128)(2,1)}), bf16[32,8,512]{2,1,0:T(8,128)(2,1)S(1)}, u32[]{:S(2)}, u32[]{:S(2)}) async-start(bf16[32,8,512]{2,1,0:T(8,128)(2,1)} %bitcast.6), calls=%async_computation | async-start | bytes 524288 | tf_op jit(solution)/shard_map/all_to_all | solution.py:232
  15.3 1.3 %collective-permute-start.7 = (bf16[1376,128]{1,0:T(8,128)(2,1)S(1)}, bf16[1376,128]{1,0:T(8,128)(2,1)S(1)}, u32[]{:S(2)}, u32[]{:S(2)}) collective-permute-start(bf16[1376,128]{1,0:T(8,128)(2,1)S(1)} %bitcast.26), channel_id=1, source_target_pairs={{0,8},{8,16},{16,24},{24,0},{1,9},{9,17},{17,25},{25,1},{2,10},{10... | collective-permute-start | bytes 1056776 | tf_op jit(solution)/shard_map/ppermute | solution.py:216
  16.6 1.4 %collective-permute-start.11 = (bf16[1376,128]{1,0:T(8,128)(2,1)S(1)}, bf16[1376,128]{1,0:T(8,128)(2,1)S(1)}, u32[]{:S(2)}, u32[]{:S(2)}) collective-permute-start(bf16[1376,128]{1,0:T(8,128)(2,1)S(1)} %bitcast.29), channel_id=1, source_target_pairs={{0,24},{8,0},{16,8},{24,16},{1,25},{9,1},{17,9},{25,17},{2,26},{10... | collective-permute-start | bytes 1056776 | tf_op jit(solution)/shard_map/ppermute | solution.py:216
  18.1 1.5 %collective-permute-start.2 = (bf16[400,128]{1,0:T(8,128)(2,1)S(1)}, bf16[400,128]{1,0:T(8,128)(2,1)S(1)}, u32[]{:S(2)}, u32[]{:S(2)}) collective-permute-start(bf16[400,128]{1,0:T(8,128)(2,1)S(1)} %get-tuple-element.22.refs_1_.refs_4_), channel_id=1, source_target_pairs={{0,16},{8,24},{16,0},{24,8},{1,17},{9,25},{17,1},{25,9},{2,18},{10... | collective-permute-start | bytes 307208 | tf_op jit(solution)/shard_map/ppermute | solution.py:216
  19.6 0.9 collective-permute-start.1
  21.1 10.1 %collective-permute-done.2.refs_4_.refs_7_ = bf16[400,128]{1,0:T(8,128)(2,1)S(1)} collective-permute-done((bf16[400,128]{1,0:T(8,128)(2,1)S(1)}, bf16[400,128]{1,0:T(8,128)(2,1)S(1)}, u32[]{:S(2)}, u32[]{:S(2)}) %collective-permute-start.2) | collective-permute-done | bytes 102432 | tf_op jit(solution)/shard_map/ppermute | solution.py:216
  31.1 1.3 %collective-permute-start.8 = (bf16[1376,128]{1,0:T(8,128)(2,1)S(1)}, bf16[1376,128]{1,0:T(8,128)(2,1)S(1)}, u32[]{:S(2)}, u32[]{:S(2)}) collective-permute-start(bf16[1376,128]{1,0:T(8,128)(2,1)S(1)} %bitcast.27), channel_id=1, source_target_pairs={{0,24},{8,0},{16,8},{24,16},{1,25},{9,1},{17,9},{25,17},{2,26},{10... | collective-permute-start | bytes 1056776 | tf_op jit(solution)/shard_map/ppermute | solution.py:216
  32.6 2.0 %collective-permute-start.9 = (bf16[1376,128]{1,0:T(8,128)(2,1)S(1)}, bf16[1376,128]{1,0:T(8,128)(2,1)S(1)}, u32[]{:S(2)}, u32[]{:S(2)}) collective-permute-start(bf16[1376,128]{1,0:T(8,128)(2,1)S(1)} %collective-permute-done.7.refs_9_), channel_id=1, source_target_pairs={{0,8},{8,16},{16,24},{24,0},{1,9},{9,17},{17,25},{25,1},{2,10},{10... | collective-permute-start | bytes 1056776 | tf_op jit(solution)/shard_map/ppermute | solution.py:216
  34.5 0.7 collective-permute-start.12
  35.3 1.7 %attend.1 = (bf16[4,256]{1,0:T(4,128)(2,1)S(1)}, bf16[4,128]{1,0:T(4,128)(2,1)S(1)}, bf16[4,256]{1,0:T(4,128)(2,1)S(1)}) custom-call(bf16[32,8,512]{2,1,0:T(8,128)(2,1)S(1)} %all-to-all-done.got_ref, bf16[16,128]{1,0:T(8,128)(2,1)S(1)} %get-tuple-element.17.dw_ref, f32[1,128]{1,0:T(1,128)S(1)} %get-tuple-element.18.bias_ref, ...), custom_call_target="tpu_custom_call" | custom-call | tf_op jit(solution)/shard_map/attend/pallas_call | solution.py:280
  37.0 13.9 %all_to_all.20 = bf16[8,4,256]{2,1,0:T(4,128)(2,1)S(1)} all-to-all(bf16[8,4,256]{2,1,0:T(4,128)(2,1)S(1)} %broadcast_in_dim.38), channel_id=1, replica_groups=mesh['z'=8,'y'=4,'x'=4,'c'=2] {'z'}, dimensions={0} | all-to-all | bytes 32768 | tf_op jit(solution)/shard_map/all_to_all | solution.py:227
  51.1 3.8 %collective-permute-start.3 = (bf16[32,512]{1,0:T(8,128)(2,1)S(1)}, bf16[32,512]{1,0:T(8,128)(2,1)S(1)}, u32[]{:S(2)}, u32[]{:S(2)}) collective-permute-start(bf16[32,512]{1,0:T(8,128)(2,1)S(1)} %shard_map.212), channel_id=1, source_target_pairs={{0,1},{1,0},{2,3},{3,2},{4,5},{5,4},{6,7},{7,6},{8,9},{9,8},{10,11... | collective-permute-start | bytes 98312 | tf_op jit(solution)/shard_map/ppermute | solution.py:216
  54.9 0.9 collective-permute-done.3
  55.8 2.8 %collective-permute-start.6 = (bf16[32,512]{1,0:T(8,128)(2,1)S(1)}, bf16[32,512]{1,0:T(8,128)(2,1)S(1)}, u32[]{:S(2)}, u32[]{:S(2)}) collective-permute-start(bf16[32,512]{1,0:T(8,128)(2,1)S(1)} %add_convert_fusion.2.refs_0_), channel_id=1, source_target_pairs={{0,4},{2,6},{4,0},{6,2},{1,5},{3,7},{5,1},{7,3},{8,12},{10,14},{12... | collective-permute-start | bytes 98312 | tf_op jit(solution)/shard_map/ppermute | solution.py:216
  58.6 0.9 collective-permute-start.5
  59.5 0.6 collective-permute-start.4
  60.2 1.2 %collective-permute-done.5.refs_2_ = bf16[32,512]{1,0:T(8,128)(2,1)S(1)} collective-permute-done((bf16[32,512]{1,0:T(8,128)(2,1)S(1)}, bf16[32,512]{1,0:T(8,128)(2,1)S(1)}, u32[]{:S(2)}, u32[]{:S(2)}) %collective-permute-start.5) | collective-permute-done | bytes 32800 | tf_op jit(solution)/shard_map/ppermute | solution.py:216
  61.4 2.1 %collective-permute-done.4.refs_1_ = bf16[32,512]{1,0:T(8,128)(2,1)S(1)} collective-permute-done((bf16[32,512]{1,0:T(8,128)(2,1)S(1)}, bf16[32,512]{1,0:T(8,128)(2,1)S(1)}, u32[]{:S(2)}, u32[]{:S(2)}) %collective-permute-start.4) | collective-permute-done | bytes 32800 | tf_op jit(solution)/shard_map/ppermute | solution.py:216
  63.5 1.2 %shard_map.213 = (bf16[4,32,128]{2,1,0:T(8,128)(2,1)S(1)}, bf16[4,2,8,1408]{3,2,1,0:T(8,128)(2,1)S(1)}) custom-call(bf16[32,512]{1,0:T(8,128)(2,1)S(1)} %add_convert_fusion.2.refs_0_, bf16[32,512]{1,0:T(8,128)(2,1)S(1)} %collective-permute-done.4.refs_1_, bf16[32,512]{1,0:T(8,128)(2,1)S(1)} %collective-permute-done.5.refs_2_, ...), custom_call_target="tpu_custom_call" | custom-call | tf_op jit(solution)/shard_map/pallas_call | solution.py:44
  64.7 10.9 %all_to_all.21.refs_0_ = bf16[8,8,1408]{2,1,0:T(8,128)(2,1)S(1)} all-to-all(bf16[8,8,1408]{2,1,0:T(8,128)(2,1)S(1)} %bitcast.32), channel_id=1, replica_groups=mesh['z'=8,'y'=4,'x'=4,'c'=2] {'z'}, dimensions={0} | all-to-all | bytes 360448 | tf_op jit(solution)/shard_map/all_to_all | solution.py:232
  75.7 0.8 broadcast_in_dim.39
  76.5 3.9 %all-to-all-start.3 = ((bf16[32,4,1408]{2,1,0:T(4,128)(2,1)}), bf16[32,4,1408]{2,1,0:T(4,128)(2,1)S(1)}, u32[]{:S(2)}, u32[]{:S(2)}) async-start(bf16[32,4,1408]{2,1,0:T(4,128)(2,1)} %broadcast_in_dim.39), calls=%async_computation.3 | async-start | bytes 720896 | tf_op jit(solution)/shard_map/all_to_all | solution.py:227
  80.4 2.9 %collective-permute-start.15 = (bf16[32,128]{1,0:T(8,128)(2,1)S(1)}, bf16[32,128]{1,0:T(8,128)(2,1)S(1)}, u32[]{:S(2)}, u32[]{:S(2)}) collective-permute-start(bf16[32,128]{1,0:T(8,128)(2,1)S(1)} %get-tuple-element.29), channel_id=1, source_target_pairs={{0,16},{8,24},{16,0},{24,8},{1,17},{9,25},{17,1},{25,9},{2,18},{10... | collective-permute-start | bytes 24584 | tf_op jit(solution)/shard_map/ppermute | solution.py:216
  83.3 0.9 collective-permute-start.14
  84.8 7.1 %all-to-all-done.3 = bf16[32,4,1408]{2,1,0:T(4,128)(2,1)S(1)} async-done(((bf16[32,4,1408]{2,1,0:T(4,128)(2,1)}), bf16[32,4,1408]{2,1,0:T(4,128)(2,1)S(1)}, u32[]{:S(2)}, u32[]{:S(2)}) %all-to-all-start.3) | async-done | bytes 360480 | tf_op jit(solution)/shard_map/all_to_all | solution.py:227
  92.2 4.6 %collective-permute-start.16 = (bf16[128,128]{1,0:T(8,128)(2,1)S(1)}, bf16[128,128]{1,0:T(8,128)(2,1)S(1)}, u32[]{:S(2)}, u32[]{:S(2)}) collective-permute-start(bf16[128,128]{1,0:T(8,128)(2,1)S(1)} %get-tuple-element.26), channel_id=1, source_target_pairs={{0,1},{1,0},{2,3},{3,2},{4,5},{5,4},{6,7},{7,6},{8,9},{9,8},{10,11... | collective-permute-start | bytes 98312 | tf_op jit(solution)/shard_map/ppermute | solution.py:216
  96.9 0.9 collective-permute-done.16
  98.0 1.3 %collective-permute-start.18 = (bf16[128,128]{1,0:T(8,128)(2,1)S(1)}, bf16[128,128]{1,0:T(8,128)(2,1)S(1)}, u32[]{:S(2)}, u32[]{:S(2)}) collective-permute-start(bf16[128,128]{1,0:T(8,128)(2,1)S(1)} %add_convert_fusion.1), channel_id=1, source_target_pairs={{0,2},{2,4},{4,6},{6,0},{1,3},{3,5},{5,7},{7,1},{8,10},{10,12},{12... | collective-permute-start | bytes 98312 | tf_op jit(solution)/shard_map/ppermute | solution.py:216
  100.9 1.1 %collective-permute-done.18 = bf16[128,128]{1,0:T(8,128)(2,1)S(1)} collective-permute-done((bf16[128,128]{1,0:T(8,128)(2,1)S(1)}, bf16[128,128]{1,0:T(8,128)(2,1)S(1)}, u32[]{:S(2)}, u32[]{:S(2)}) %collective-permute-start.18) | collective-permute-done | bytes 32800 | tf_op jit(solution)/shard_map/ppermute | solution.py:216
  102.0 1.6 %collective-permute-done.17 = bf16[128,128]{1,0:T(8,128)(2,1)S(1)} collective-permute-done((bf16[128,128]{1,0:T(8,128)(2,1)S(1)}, bf16[128,128]{1,0:T(8,128)(2,1)S(1)}, u32[]{:S(2)}, u32[]{:S(2)}) %collective-permute-start.17) | collective-permute-done | bytes 32800 | tf_op jit(solution)/shard_map/ppermute | solution.py:216
  103.6 0.6 add_convert_fusion
  (36 shorter events, 3.9 us)
Async XLA Ops:
  0.6 14.7 %copy-start = (bf16[128,1376]{0,1:T(8,128)(2,1)S(1)}, bf16[128,1376]{0,1:T(8,128)(2,1)}, u32[]{:S(2)}) copy-start(bf16[128,1376]{0,1:T(8,128)(2,1)} %param.37) | copy-start | bytes 1056772
  0.6 16.0 %copy-start.1 = (bf16[128,1376]{0,1:T(8,128)(2,1)S(1)}, bf16[128,1376]{0,1:T(8,128)(2,1)}, u32[]{:S(2)}) copy-start(bf16[128,1376]{0,1:T(8,128)(2,1)} %param.38) | copy-start | bytes 1056772
  3.2 32.0 %all-to-all-start = ((bf16[32,8,512]{2,1,0:T(8,128)(2,1)}), bf16[32,8,512]{2,1,0:T(8,128)(2,1)S(1)}, u32[]{:S(2)}, u32[]{:S(2)}) async-start(bf16[32,8,512]{2,1,0:T(8,128)(2,1)} %bitcast.6), calls=%async_computation | async-start | bytes 524288 | tf_op jit(solution)/shard_map/all_to_all | solution.py:232
  15.3 17.3 %collective-permute-start.7 = (bf16[1376,128]{1,0:T(8,128)(2,1)S(1)}, bf16[1376,128]{1,0:T(8,128)(2,1)S(1)}, u32[]{:S(2)}, u32[]{:S(2)}) collective-permute-start(bf16[1376,128]{1,0:T(8,128)(2,1)S(1)} %bitcast.26), channel_id=1, source_target_pairs={{0,8},{8,16},{16,24},{24,0},{1,9},{9,17},{17,25},{25,1},{2,10},{10... | collective-permute-start | bytes 1056776 | tf_op jit(solution)/shard_map/ppermute | solution.py:216
  16.6 17.9 %collective-permute-start.11 = (bf16[1376,128]{1,0:T(8,128)(2,1)S(1)}, bf16[1376,128]{1,0:T(8,128)(2,1)S(1)}, u32[]{:S(2)}, u32[]{:S(2)}) collective-permute-start(bf16[1376,128]{1,0:T(8,128)(2,1)S(1)} %bitcast.29), channel_id=1, source_target_pairs={{0,24},{8,0},{16,8},{24,16},{1,25},{9,1},{17,9},{25,17},{2,26},{10... | collective-permute-start | bytes 1056776 | tf_op jit(solution)/shard_map/ppermute | solution.py:216
  18.1 13.0 %collective-permute-start.2 = (bf16[400,128]{1,0:T(8,128)(2,1)S(1)}, bf16[400,128]{1,0:T(8,128)(2,1)S(1)}, u32[]{:S(2)}, u32[]{:S(2)}) collective-permute-start(bf16[400,128]{1,0:T(8,128)(2,1)S(1)} %get-tuple-element.22.refs_1_.refs_4_), channel_id=1, source_target_pairs={{0,16},{8,24},{16,0},{24,8},{1,17},{9,25},{17,1},{25,9},{2,18},{10... | collective-permute-start | bytes 307208 | tf_op jit(solution)/shard_map/ppermute | solution.py:216
  19.6 12.9 %collective-permute-start.1 = (bf16[400,128]{1,0:T(8,128)(2,1)S(1)}, bf16[400,128]{1,0:T(8,128)(2,1)S(1)}, u32[]{:S(2)}, u32[]{:S(2)}) collective-permute-start(bf16[400,128]{1,0:T(8,128)(2,1)S(1)} %get-tuple-element.22.refs_1_.refs_4_), channel_id=1, source_target_pairs={{0,24},{8,0},{16,8},{24,16},{1,25},{9,1},{17,9},{25,17},{2,26},{10... | collective-permute-start | bytes 307208 | tf_op jit(solution)/shard_map/ppermute | solution.py:216
  20.5 30.5 %collective-permute-start = (bf16[400,128]{1,0:T(8,128)(2,1)S(1)}, bf16[400,128]{1,0:T(8,128)(2,1)S(1)}, u32[]{:S(2)}, u32[]{:S(2)}) collective-permute-start(bf16[400,128]{1,0:T(8,128)(2,1)S(1)} %get-tuple-element.22.refs_1_.refs_4_), channel_id=1, source_target_pairs={{0,8},{8,16},{16,24},{24,0},{1,9},{9,17},{17,25},{25,1},{2,10},{10... | collective-permute-start | bytes 307208 | tf_op jit(solution)/shard_map/ppermute | solution.py:216
  31.1 27.5 %collective-permute-start.8 = (bf16[1376,128]{1,0:T(8,128)(2,1)S(1)}, bf16[1376,128]{1,0:T(8,128)(2,1)S(1)}, u32[]{:S(2)}, u32[]{:S(2)}) collective-permute-start(bf16[1376,128]{1,0:T(8,128)(2,1)S(1)} %bitcast.27), channel_id=1, source_target_pairs={{0,24},{8,0},{16,8},{24,16},{1,25},{9,1},{17,9},{25,17},{2,26},{10... | collective-permute-start | bytes 1056776 | tf_op jit(solution)/shard_map/ppermute | solution.py:216
  32.5 27.0 %collective-permute-start.10 = (bf16[1376,128]{1,0:T(8,128)(2,1)S(1)}, bf16[1376,128]{1,0:T(8,128)(2,1)S(1)}, u32[]{:S(2)}, u32[]{:S(2)}) collective-permute-start(bf16[1376,128]{1,0:T(8,128)(2,1)S(1)} %bitcast.30), channel_id=1, source_target_pairs={{0,8},{8,16},{16,24},{24,0},{1,9},{9,17},{17,25},{25,1},{2,10},{10... | collective-permute-start | bytes 1056776 | tf_op jit(solution)/shard_map/ppermute | solution.py:216
  32.6 30.9 %collective-permute-start.9 = (bf16[1376,128]{1,0:T(8,128)(2,1)S(1)}, bf16[1376,128]{1,0:T(8,128)(2,1)S(1)}, u32[]{:S(2)}, u32[]{:S(2)}) collective-permute-start(bf16[1376,128]{1,0:T(8,128)(2,1)S(1)} %collective-permute-done.7.refs_9_), channel_id=1, source_target_pairs={{0,8},{8,16},{16,24},{24,0},{1,9},{9,17},{17,25},{25,1},{2,10},{10... | collective-permute-start | bytes 1056776 | tf_op jit(solution)/shard_map/ppermute | solution.py:216
  34.5 29.0 %collective-permute-start.12 = (bf16[1376,128]{1,0:T(8,128)(2,1)S(1)}, bf16[1376,128]{1,0:T(8,128)(2,1)S(1)}, u32[]{:S(2)}, u32[]{:S(2)}) collective-permute-start(bf16[1376,128]{1,0:T(8,128)(2,1)S(1)} %collective-permute-done.11.refs_14_), channel_id=1, source_target_pairs={{0,24},{8,0},{16,8},{24,16},{1,25},{9,1},{17,9},{25,17},{2,26},{10... | collective-permute-start | bytes 1056776 | tf_op jit(solution)/shard_map/ppermute | solution.py:216
  51.1 4.7 %collective-permute-start.3 = (bf16[32,512]{1,0:T(8,128)(2,1)S(1)}, bf16[32,512]{1,0:T(8,128)(2,1)S(1)}, u32[]{:S(2)}, u32[]{:S(2)}) collective-permute-start(bf16[32,512]{1,0:T(8,128)(2,1)S(1)} %shard_map.212), channel_id=1, source_target_pairs={{0,1},{1,0},{2,3},{3,2},{4,5},{5,4},{6,7},{7,6},{8,9},{9,8},{10,11... | collective-permute-start | bytes 98312 | tf_op jit(solution)/shard_map/ppermute | solution.py:216
  55.8 4.4 %collective-permute-start.6 = (bf16[32,512]{1,0:T(8,128)(2,1)S(1)}, bf16[32,512]{1,0:T(8,128)(2,1)S(1)}, u32[]{:S(2)}, u32[]{:S(2)}) collective-permute-start(bf16[32,512]{1,0:T(8,128)(2,1)S(1)} %add_convert_fusion.2.refs_0_), channel_id=1, source_target_pairs={{0,4},{2,6},{4,0},{6,2},{1,5},{3,7},{5,1},{7,3},{8,12},{10,14},{12... | collective-permute-start | bytes 98312 | tf_op jit(solution)/shard_map/ppermute | solution.py:216
  58.6 2.8 %collective-permute-start.5 = (bf16[32,512]{1,0:T(8,128)(2,1)S(1)}, bf16[32,512]{1,0:T(8,128)(2,1)S(1)}, u32[]{:S(2)}, u32[]{:S(2)}) collective-permute-start(bf16[32,512]{1,0:T(8,128)(2,1)S(1)} %add_convert_fusion.2.refs_0_), channel_id=1, source_target_pairs={{0,6},{2,0},{4,2},{6,4},{1,7},{3,1},{5,3},{7,5},{8,14},{10,8},{12,... | collective-permute-start | bytes 98312 | tf_op jit(solution)/shard_map/ppermute | solution.py:216
  59.5 4.0 %collective-permute-start.4 = (bf16[32,512]{1,0:T(8,128)(2,1)S(1)}, bf16[32,512]{1,0:T(8,128)(2,1)S(1)}, u32[]{:S(2)}, u32[]{:S(2)}) collective-permute-start(bf16[32,512]{1,0:T(8,128)(2,1)S(1)} %add_convert_fusion.2.refs_0_), channel_id=1, source_target_pairs={{0,2},{2,4},{4,6},{6,0},{1,3},{3,5},{5,7},{7,1},{8,10},{10,12},{12... | collective-permute-start | bytes 98312 | tf_op jit(solution)/shard_map/ppermute | solution.py:216
  76.5 15.3 %all-to-all-start.3 = ((bf16[32,4,1408]{2,1,0:T(4,128)(2,1)}), bf16[32,4,1408]{2,1,0:T(4,128)(2,1)S(1)}, u32[]{:S(2)}, u32[]{:S(2)}) async-start(bf16[32,4,1408]{2,1,0:T(4,128)(2,1)} %broadcast_in_dim.39), calls=%async_computation.3 | async-start | bytes 720896 | tf_op jit(solution)/shard_map/all_to_all | solution.py:227
  80.4 11.5 %collective-permute-start.15 = (bf16[32,128]{1,0:T(8,128)(2,1)S(1)}, bf16[32,128]{1,0:T(8,128)(2,1)S(1)}, u32[]{:S(2)}, u32[]{:S(2)}) collective-permute-start(bf16[32,128]{1,0:T(8,128)(2,1)S(1)} %get-tuple-element.29), channel_id=1, source_target_pairs={{0,16},{8,24},{16,0},{24,8},{1,17},{9,25},{17,1},{25,9},{2,18},{10... | collective-permute-start | bytes 24584 | tf_op jit(solution)/shard_map/ppermute | solution.py:216
  83.3 8.7 %collective-permute-start.14 = (bf16[32,128]{1,0:T(8,128)(2,1)S(1)}, bf16[32,128]{1,0:T(8,128)(2,1)S(1)}, u32[]{:S(2)}, u32[]{:S(2)}) collective-permute-start(bf16[32,128]{1,0:T(8,128)(2,1)S(1)} %get-tuple-element.30), channel_id=1, source_target_pairs={{0,24},{8,0},{16,8},{24,16},{1,25},{9,1},{17,9},{25,17},{2,26},{10... | collective-permute-start | bytes 24584 | tf_op jit(solution)/shard_map/ppermute | solution.py:216
  84.2 7.8 %copy-start.2 = (bf16[1376,128]{1,0:T(8,128)(2,1)S(1)}, bf16[1376,128]{1,0:T(8,128)(2,1)}, u32[]{:S(2)}) copy-start(bf16[1376,128]{1,0:T(8,128)(2,1)} %refs_1_.1) | copy-start | bytes 1056772
  84.2 7.8 %collective-permute-start.13 = (bf16[32,128]{1,0:T(8,128)(2,1)S(1)}, bf16[32,128]{1,0:T(8,128)(2,1)S(1)}, u32[]{:S(2)}, u32[]{:S(2)}) collective-permute-start(bf16[32,128]{1,0:T(8,128)(2,1)S(1)} %get-tuple-element.31), channel_id=1, source_target_pairs={{0,8},{8,16},{16,24},{24,0},{1,9},{9,17},{17,25},{25,1},{2,10},{10... | collective-permute-start | bytes 24584 | tf_op jit(solution)/shard_map/ppermute | solution.py:216
  92.2 5.5 %collective-permute-start.16 = (bf16[128,128]{1,0:T(8,128)(2,1)S(1)}, bf16[128,128]{1,0:T(8,128)(2,1)S(1)}, u32[]{:S(2)}, u32[]{:S(2)}) collective-permute-start(bf16[128,128]{1,0:T(8,128)(2,1)S(1)} %get-tuple-element.26), channel_id=1, source_target_pairs={{0,1},{1,0},{2,3},{3,2},{4,5},{5,4},{6,7},{7,6},{8,9},{9,8},{10,11... | collective-permute-start | bytes 98312 | tf_op jit(solution)/shard_map/ppermute | solution.py:216
  97.7 3.1 %collective-permute-start.19 = (bf16[128,128]{1,0:T(8,128)(2,1)S(1)}, bf16[128,128]{1,0:T(8,128)(2,1)S(1)}, u32[]{:S(2)}, u32[]{:S(2)}) collective-permute-start(bf16[128,128]{1,0:T(8,128)(2,1)S(1)} %add_convert_fusion.1), channel_id=1, source_target_pairs={{0,6},{2,0},{4,2},{6,4},{1,7},{3,1},{5,3},{7,5},{8,14},{10,8},{12,... | collective-permute-start | bytes 98312 | tf_op jit(solution)/shard_map/ppermute | solution.py:216
  98.0 4.0 %collective-permute-start.18 = (bf16[128,128]{1,0:T(8,128)(2,1)S(1)}, bf16[128,128]{1,0:T(8,128)(2,1)S(1)}, u32[]{:S(2)}, u32[]{:S(2)}) collective-permute-start(bf16[128,128]{1,0:T(8,128)(2,1)S(1)} %add_convert_fusion.1), channel_id=1, source_target_pairs={{0,2},{2,4},{4,6},{6,0},{1,3},{3,5},{5,7},{7,1},{8,10},{10,12},{12... | collective-permute-start | bytes 98312 | tf_op jit(solution)/shard_map/ppermute | solution.py:216
  99.3 4.3 %collective-permute-start.17 = (bf16[128,128]{1,0:T(8,128)(2,1)S(1)}, bf16[128,128]{1,0:T(8,128)(2,1)S(1)}, u32[]{:S(2)}, u32[]{:S(2)}) collective-permute-start(bf16[128,128]{1,0:T(8,128)(2,1)S(1)} %add_convert_fusion.1), channel_id=1, source_target_pairs={{0,4},{2,6},{4,0},{6,2},{1,5},{3,7},{5,1},{7,3},{8,12},{10,14},{12... | collective-permute-start | bytes 98312 | tf_op jit(solution)/shard_map/ppermute | solution.py:216

commit v3 on v2

--- a/solution.py
+++ b/solution.py
@@ -13,9 +13,9 @@
 TP = ("x", "c")
 F32 = jnp.float32
 BF16 = jnp.bfloat16
-FIRST = 512
-CODE_AT = 256
-SQUARE_AT = 272
+FIRST = 896
+CODE_AT = 768
+SQUARE_AT = 784
 TOKENS_AT = 256
 GAIN_AT = 384
 SENT = 400
@@ -80,13 +80,13 @@
     scaled = (tok * gain_ref[...]).astype(BF16)
     squares = jnp.sum(tok * tok, axis=1, keepdims=True)
     code = dot(scaled, code_ref[...], ((1,), (1,)))
-    lane = lax.broadcasted_iota(jnp.int32, (128, 256), 1)
-    tail = jnp.concatenate([code, jnp.zeros((128, 240), F32)], axis=1)
+    lane = lax.broadcasted_iota(jnp.int32, (128, 128), 1)
+    tail = jnp.concatenate([code, jnp.zeros((128, 112), F32)], axis=1)
     tail = jnp.where(lane == SQUARE_AT - CODE_AT, squares, tail)
-    out_gate = dot(scaled, g_ref[...])
-    head = jnp.concatenate([dot(scaled, q_ref[...]), dot(scaled, k_ref[...])], axis=1)
-    store_shares(out_ref, head, out_gate)
-    store_shares(out_ref, dot(scaled, v_ref[...]), tail, 256)
+    products = [dot(scaled, ref[...]) for ref in (q_ref, k_ref, v_ref, g_ref)]
+    every = jnp.concatenate([*products, tail], axis=1).astype(BF16)
+    for share in range(32):
+        out_ref[share] = every[4 * share : 4 * share + 4]
 
 
 def rounded(x):
@@ -103,16 +103,13 @@
     for copy in copies:
         copy.start()
     total = jnp.sum(got_ref[...].astype(F32), axis=0)
-    squares = jnp.broadcast_to(total[:, SQUARE_AT : SQUARE_AT + 1], (8, 128))
-    inv_high = lax.rsqrt(squares / WIDTH + EPS)
-    inv_low = pltpu.roll(inv_high, 4, 0)
-    twice = lambda x: jnp.concatenate([x, x], axis=1)
-    queries = rounded(total[:, 0:128] * inv_low * 128 ** (-0.5))
-    keys = (total[:, 128:256] * inv_low).astype(BF16)
-    values = (total[:, 256:512] * twice(inv_low)).astype(BF16)
-    out_gate = pltpu.roll(rounded(total[:, 0:256] * twice(inv_high)), 4, 0)
-    code = (total[:, CODE_AT : CODE_AT + 128] * inv_high).astype(BF16)[:, 0:16]
-    pre = pltpu.roll(dot(code, dw_ref[...]) + bias_ref[...], 4, 0)
+    inv = lax.rsqrt(total[:, SQUARE_AT : SQUARE_AT + 1] / WIDTH + EPS)
+    queries = rounded(total[:, 0:128] * inv * 128 ** (-0.5))
+    keys = (total[:, 128:256] * inv).astype(BF16)
+    values = (total[:, 256:512] * inv).astype(BF16)
+    gate = rounded(total[:, 512:768] * inv)
+    code = (total[:, CODE_AT : CODE_AT + 128] * inv).astype(BF16)[:, 0:16]
+    pre = dot(code, dw_ref[...]) + bias_ref[...]
     log_sig = jnp.minimum(pre, 0.0) - jnp.log1p(jnp.exp(-jnp.abs(pre)))
     decayed = queries * jnp.exp(log_sig / GATE_TEMP)
     own = jnp.sum(queries * keys.astype(F32), axis=1, keepdims=True)
@@ -125,7 +122,7 @@
     kept = [jnp.where(live[b], decay_ref[b], 0.0) for b in range(4)]
     sums = dot(later, jnp.concatenate(kept, axis=1), precision=lax.Precision.HIGHEST)
     totals = jnp.concatenate([jnp.sum(k, axis=0, keepdims=True) for k in kept], axis=0)
-    carry = decayed[0:4] * jnp.exp(totals)
+    carry = decayed * jnp.exp(totals)
     columns = jnp.concatenate([carry, carry], axis=0).T
     for copy in copies[1:]:
         copy.wait()
@@ -136,12 +133,11 @@
         within = jnp.sum(rounded(scores) * value_ref[b].astype(F32), axis=0, keepdims=True)
         carried = jnp.sum(columns[:, b : b + 1] * state_ref[b], axis=0, keepdims=True)
         mixed.append(carried + within)
-    mixed = jnp.concatenate(mixed, axis=0) + own[0:4] * values[0:4].astype(F32)
+    mixed = jnp.concatenate(mixed, axis=0) + own * values.astype(F32)
     scale = lax.rsqrt(jnp.mean(mixed * mixed, axis=1, keepdims=True) + EPS)
-    gate = out_gate[0:4]
     heads_ref[...] = (mixed * scale * hg_ref[...] * (gate / (1.0 + jnp.exp(-gate)))).astype(BF16)
-    nk_ref[...] = keys[0:4]
-    nv_ref[...] = values[0:4]
+    nk_ref[...] = keys
+    nv_ref[...] = values
 
 
 def sequences_of(y, shape, dim):
@@ -170,12 +166,12 @@
         mid_ref[k] = middle[:, 128 * k : 128 * k + 128]
         gain = jnp.sum(ref[GAIN_AT:SENT, :].astype(F32), axis=0, keepdims=True)
         scaled.append((mid[:, 128 * k : 128 * k + 128] * gain).astype(BF16))
+    scaled = [jnp.concatenate(scaled[k : k + 2], axis=1) for k in (0, 2)]
     squares = jnp.sum(mid * mid, axis=1, keepdims=True)
 
     def product(weights, at, size):
-        return sum(
-            dot(part, ref[at : at + size, :], ((1,), (1,))) for part, ref in zip(scaled, weights)
-        )
+        pairs = [jnp.concatenate([ref[at : at + size, :] for ref in weights[k : k + 2]], axis=1) for k in (0, 2)]
+        return sum(dot(part, pair, ((1,), (1,))) for part, pair in zip(scaled, pairs))
 
     for at, width in ((0, 512), (512, 512), (1024, 384)):
         real = min(width, UNITS - at)
@@ -229,7 +225,7 @@
 
 
 def shares(x, axes):
-    return lax.all_to_all(x.reshape(-1, 8, x.shape[-1]), axes, 0, 0, tiled=True)
+    return lax.all_to_all(x, axes, 0, 0, tiled=True)
 
 
 def layer(
@@ -261,7 +257,7 @@
     first, sent, *small = kernel(
         project_body,
         [
-            ((32 // 2, 2, 8, FIRST), BF16),
+            ((32, 4, FIRST), BF16),
             ((SENT, 128), BF16),
             *((a.shape, a.dtype) for a in small),
         ],
@@ -296,7 +292,7 @@
     middle, second = kernel(
         lift_body, [((4, 32, 128), BF16), ((4, 2, 8, SECOND), BF16)], (*tp_parts(attended), *sent, *gates, *ups)
     )
-    (hidden,) = kernel(hidden_body, [((seqs, SECOND), BF16)], (shares(second, "z"),))
+    (hidden,) = kernel(hidden_body, [((seqs, SECOND), BF16)], (shares(second.reshape(8, 8, SECOND), "z"),))
     middles = (middle[0], moved(middle[2], "y", 1), moved(middle[1], "y", 3), moved(middle[3], "y", 2))
     lifted, middle = kernel(
         down_body, [((128, 128), BF16), ((128, 128), BF16)], (to_all(hidden, KV), down_weight, *middles)

time: 105 us -> 104 us (level)
  transfers between devices with their start and end apart: 22 -> 22, of which waited for: 10 -> 9; matrix products, arithmetic and copies ran while one was open for 1% -> 1% of each run, Pallas kernels for 2% -> 2%
where the time goes in v3:
time: 104 us
  starting transfers between devices  44.8 us (43%)
  blocking collectives  24.8 us (24%)
  waiting for transfers between devices  24.7 us (24%)
  Pallas kernels  5.83 us (6%)
  local copies, waits for them, and re-layouts  2.1 us (2%)
    ppermute x20, starting transfers between devices, moved(): lax.ppermute(x, axis, [(i, (i + shift) % length) for i in range(length)])  28.9 us
    ppermute x20, waiting for transfers between devices, moved(): lax.ppermute(x, axis, [(i, (i + shift) % length) for i in range(length)])  17.6 us
    all_to_all x1, blocking collectives, to_all(): got = lax.all_to_all(copies, axes, 0, 0, tiled=True)  13.9 us
    all_to_all x1, starting transfers between devices, shares(): return lax.all_to_all(x, axes, 0, 0, tiled=True)  12 us
    all_to_all x1, blocking collectives, shares(): return lax.all_to_all(x, axes, 0, 0, tiled=True)  10.9 us
    all_to_all x1, waiting for transfers between devices, to_all(): got = lax.all_to_all(copies, axes, 0, 0, tiled=True)  7.09 us
    pallas_call x5, Pallas kernels, kernel(): pl.pallas_call(whole, out_shape=tuple((pltpu.VMEM(*out) for out in outs))...  4.07 us
    all_to_all x1, starting transfers between devices, to_all(): got = lax.all_to_all(copies, axes, 0, 0, tiled=True)  3.88 us
  transfers between devices with their start and end apart: 22, of which 9 were waited for; matrix products, arithmetic and copies ran while one was open for 1% of the time, Pallas kernels for 2%

profile of v3, /device:TPU:1, one launch (start us, length us, event | category | flops | bytes accessed | tf_op | source)
XLA Modules:
  0.0 103.7 jit_solution(1975387030783318476)
XLA Ops:
  0.7 2.6 %shard_map.211 = (bf16[32,4,896]{2,1,0:T(4,128)(2,1)}, bf16[400,128]{1,0:T(8,128)(2,1)S(1)}, bf16[16,128]{1,0:T(8,128)(2,1)S(1)}, f32[1,128]{1,0:T(1,128)S(1)}, ...) custom-call(bf16[128,128]{1,0:T(8,128)(2,1)} %refs_9_.1, f32[1,128]{1,0:T(1,128)} %bitcast.38, bf16[128,128]{1,0:T(8,128)(2,1)} %refs_2_.1, ...), custom_call_target="tpu_custom_call" | custom-call | tf_op jit(solution)/shard_map/pallas_call | solution.py:44
  3.2 12.0 %all-to-all-start = ((bf16[32,4,896]{2,1,0:T(4,128)(2,1)}), bf16[32,4,896]{2,1,0:T(4,128)(2,1)S(1)}, u32[]{:S(2)}, u32[]{:S(2)}) async-start(bf16[32,4,896]{2,1,0:T(4,128)(2,1)} %get-tuple-element.16), calls=%async_computation | async-start | bytes 458752 | tf_op jit(solution)/shard_map/all_to_all | solution.py:228
  15.3 1.3 %collective-permute-start.7 = (bf16[1376,128]{1,0:T(8,128)(2,1)S(1)}, bf16[1376,128]{1,0:T(8,128)(2,1)S(1)}, u32[]{:S(2)}, u32[]{:S(2)}) collective-permute-start(bf16[1376,128]{1,0:T(8,128)(2,1)S(1)} %bitcast.25), channel_id=1, source_target_pairs={{0,8},{8,16},{16,24},{24,0},{1,9},{9,17},{17,25},{25,1},{2,10},{10... | collective-permute-start | bytes 1056776 | tf_op jit(solution)/shard_map/ppermute | solution.py:212
  16.6 1.4 %collective-permute-start.11 = (bf16[1376,128]{1,0:T(8,128)(2,1)S(1)}, bf16[1376,128]{1,0:T(8,128)(2,1)S(1)}, u32[]{:S(2)}, u32[]{:S(2)}) collective-permute-start(bf16[1376,128]{1,0:T(8,128)(2,1)S(1)} %bitcast.28), channel_id=1, source_target_pairs={{0,24},{8,0},{16,8},{24,16},{1,25},{9,1},{17,9},{25,17},{2,26},{10... | collective-permute-start | bytes 1056776 | tf_op jit(solution)/shard_map/ppermute | solution.py:212
  18.0 1.5 %collective-permute-start.2 = (bf16[400,128]{1,0:T(8,128)(2,1)S(1)}, bf16[400,128]{1,0:T(8,128)(2,1)S(1)}, u32[]{:S(2)}, u32[]{:S(2)}) collective-permute-start(bf16[400,128]{1,0:T(8,128)(2,1)S(1)} %get-tuple-element.22.refs_1_.refs_4_), channel_id=1, source_target_pairs={{0,16},{8,24},{16,0},{24,8},{1,17},{9,25},{17,1},{25,9},{2,18},{10... | collective-permute-start | bytes 307208 | tf_op jit(solution)/shard_map/ppermute | solution.py:212
  19.6 0.9 collective-permute-start.1
  21.0 9.7 %collective-permute-done.2.refs_4_.refs_7_ = bf16[400,128]{1,0:T(8,128)(2,1)S(1)} collective-permute-done((bf16[400,128]{1,0:T(8,128)(2,1)S(1)}, bf16[400,128]{1,0:T(8,128)(2,1)S(1)}, u32[]{:S(2)}, u32[]{:S(2)}) %collective-permute-start.2) | collective-permute-done | bytes 102432 | tf_op jit(solution)/shard_map/ppermute | solution.py:212
  30.8 1.2 %collective-permute-start.8 = (bf16[1376,128]{1,0:T(8,128)(2,1)S(1)}, bf16[1376,128]{1,0:T(8,128)(2,1)S(1)}, u32[]{:S(2)}, u32[]{:S(2)}) collective-permute-start(bf16[1376,128]{1,0:T(8,128)(2,1)S(1)} %bitcast.26), channel_id=1, source_target_pairs={{0,24},{8,0},{16,8},{24,16},{1,25},{9,1},{17,9},{25,17},{2,26},{10... | collective-permute-start | bytes 1056776 | tf_op jit(solution)/shard_map/ppermute | solution.py:212
  32.3 1.9 %collective-permute-start.9 = (bf16[1376,128]{1,0:T(8,128)(2,1)S(1)}, bf16[1376,128]{1,0:T(8,128)(2,1)S(1)}, u32[]{:S(2)}, u32[]{:S(2)}) collective-permute-start(bf16[1376,128]{1,0:T(8,128)(2,1)S(1)} %collective-permute-done.7.refs_9_), channel_id=1, source_target_pairs={{0,8},{8,16},{16,24},{24,0},{1,9},{9,17},{17,25},{25,1},{2,10},{10... | collective-permute-start | bytes 1056776 | tf_op jit(solution)/shard_map/ppermute | solution.py:212
  34.2 0.8 collective-permute-start.12
  35.0 1.8 %attend.1 = (bf16[4,256]{1,0:T(4,128)(2,1)S(1)}, bf16[4,128]{1,0:T(4,128)(2,1)S(1)}, bf16[4,256]{1,0:T(4,128)(2,1)S(1)}) custom-call(bf16[32,4,896]{2,1,0:T(4,128)(2,1)S(1)} %all-to-all-done.got_ref, bf16[16,128]{1,0:T(8,128)(2,1)S(1)} %get-tuple-element.17.dw_ref, f32[1,128]{1,0:T(1,128)S(1)} %get-tuple-element.18.bias_ref, ...), custom_call_target="tpu_custom_call" | custom-call | tf_op jit(solution)/shard_map/attend/pallas_call | solution.py:276
  36.8 13.9 %all_to_all.20 = bf16[8,4,256]{2,1,0:T(4,128)(2,1)S(1)} all-to-all(bf16[8,4,256]{2,1,0:T(4,128)(2,1)S(1)} %broadcast_in_dim.38), channel_id=1, replica_groups=mesh['z'=8,'y'=4,'x'=4,'c'=2] {'z'}, dimensions={0} | all-to-all | bytes 32768 | tf_op jit(solution)/shard_map/all_to_all | solution.py:223
  50.9 3.7 %collective-permute-start.3 = (bf16[32,512]{1,0:T(8,128)(2,1)S(1)}, bf16[32,512]{1,0:T(8,128)(2,1)S(1)}, u32[]{:S(2)}, u32[]{:S(2)}) collective-permute-start(bf16[32,512]{1,0:T(8,128)(2,1)S(1)} %shard_map.212), channel_id=1, source_target_pairs={{0,1},{1,0},{2,3},{3,2},{4,5},{5,4},{6,7},{7,6},{8,9},{9,8},{10,11... | collective-permute-start | bytes 98312 | tf_op jit(solution)/shard_map/ppermute | solution.py:212
  54.6 0.9 collective-permute-done.3
  55.5 2.8 %collective-permute-start.6 = (bf16[32,512]{1,0:T(8,128)(2,1)S(1)}, bf16[32,512]{1,0:T(8,128)(2,1)S(1)}, u32[]{:S(2)}, u32[]{:S(2)}) collective-permute-start(bf16[32,512]{1,0:T(8,128)(2,1)S(1)} %add_convert_fusion.2.refs_0_), channel_id=1, source_target_pairs={{0,4},{2,6},{4,0},{6,2},{1,5},{3,7},{5,1},{7,3},{8,12},{10,14},{12... | collective-permute-start | bytes 98312 | tf_op jit(solution)/shard_map/ppermute | solution.py:212
  58.3 0.9 collective-permute-start.5
  59.2 0.6 collective-permute-start.4
  59.9 1.2 %collective-permute-done.5.refs_2_ = bf16[32,512]{1,0:T(8,128)(2,1)S(1)} collective-permute-done((bf16[32,512]{1,0:T(8,128)(2,1)S(1)}, bf16[32,512]{1,0:T(8,128)(2,1)S(1)}, u32[]{:S(2)}, u32[]{:S(2)}) %collective-permute-start.5) | collective-permute-done | bytes 32800 | tf_op jit(solution)/shard_map/ppermute | solution.py:212
  61.1 2.1 %collective-permute-done.4.refs_1_ = bf16[32,512]{1,0:T(8,128)(2,1)S(1)} collective-permute-done((bf16[32,512]{1,0:T(8,128)(2,1)S(1)}, bf16[32,512]{1,0:T(8,128)(2,1)S(1)}, u32[]{:S(2)}, u32[]{:S(2)}) %collective-permute-start.4) | collective-permute-done | bytes 32800 | tf_op jit(solution)/shard_map/ppermute | solution.py:212
  63.2 1.0 shard_map.213
  64.2 10.9 %all_to_all.21.refs_0_ = bf16[8,8,1408]{2,1,0:T(8,128)(2,1)S(1)} all-to-all(bf16[8,8,1408]{2,1,0:T(8,128)(2,1)S(1)} %bitcast.31), channel_id=1, replica_groups=mesh['z'=8,'y'=4,'x'=4,'c'=2] {'z'}, dimensions={0} | all-to-all | bytes 360448 | tf_op jit(solution)/shard_map/all_to_all | solution.py:228
  75.2 0.8 broadcast_in_dim.39
  76.0 3.9 %all-to-all-start.3 = ((bf16[32,4,1408]{2,1,0:T(4,128)(2,1)}), bf16[32,4,1408]{2,1,0:T(4,128)(2,1)S(1)}, u32[]{:S(2)}, u32[]{:S(2)}) async-start(bf16[32,4,1408]{2,1,0:T(4,128)(2,1)} %broadcast_in_dim.39), calls=%async_computation.3 | async-start | bytes 720896 | tf_op jit(solution)/shard_map/all_to_all | solution.py:223
  79.9 2.9 %collective-permute-start.15 = (bf16[32,128]{1,0:T(8,128)(2,1)S(1)}, bf16[32,128]{1,0:T(8,128)(2,1)S(1)}, u32[]{:S(2)}, u32[]{:S(2)}) collective-permute-start(bf16[32,128]{1,0:T(8,128)(2,1)S(1)} %get-tuple-element.29), channel_id=1, source_target_pairs={{0,16},{8,24},{16,0},{24,8},{1,17},{9,25},{17,1},{25,9},{2,18},{10... | collective-permute-start | bytes 24584 | tf_op jit(solution)/shard_map/ppermute | solution.py:212
  82.8 0.9 collective-permute-start.14
  84.3 7.1 %all-to-all-done.3 = bf16[32,4,1408]{2,1,0:T(4,128)(2,1)S(1)} async-done(((bf16[32,4,1408]{2,1,0:T(4,128)(2,1)}), bf16[32,4,1408]{2,1,0:T(4,128)(2,1)S(1)}, u32[]{:S(2)}, u32[]{:S(2)}) %all-to-all-start.3) | async-done | bytes 360480 | tf_op jit(solution)/shard_map/all_to_all | solution.py:223
  91.7 4.6 %collective-permute-start.16 = (bf16[128,128]{1,0:T(8,128)(2,1)S(1)}, bf16[128,128]{1,0:T(8,128)(2,1)S(1)}, u32[]{:S(2)}, u32[]{:S(2)}) collective-permute-start(bf16[128,128]{1,0:T(8,128)(2,1)S(1)} %get-tuple-element.26), channel_id=1, source_target_pairs={{0,1},{1,0},{2,3},{3,2},{4,5},{5,4},{6,7},{7,6},{8,9},{9,8},{10,11... | collective-permute-start | bytes 98312 | tf_op jit(solution)/shard_map/ppermute | solution.py:212
  96.4 0.9 collective-permute-done.16
  97.5 1.3 %collective-permute-start.18 = (bf16[128,128]{1,0:T(8,128)(2,1)S(1)}, bf16[128,128]{1,0:T(8,128)(2,1)S(1)}, u32[]{:S(2)}, u32[]{:S(2)}) collective-permute-start(bf16[128,128]{1,0:T(8,128)(2,1)S(1)} %add_convert_fusion.1), channel_id=1, source_target_pairs={{0,2},{2,4},{4,6},{6,0},{1,3},{3,5},{5,7},{7,1},{8,10},{10,12},{12... | collective-permute-start | bytes 98312 | tf_op jit(solution)/shard_map/ppermute | solution.py:212
  100.4 1.1 %collective-permute-done.18 = bf16[128,128]{1,0:T(8,128)(2,1)S(1)} collective-permute-done((bf16[128,128]{1,0:T(8,128)(2,1)S(1)}, bf16[128,128]{1,0:T(8,128)(2,1)S(1)}, u32[]{:S(2)}, u32[]{:S(2)}) %collective-permute-start.18) | collective-permute-done | bytes 32800 | tf_op jit(solution)/shard_map/ppermute | solution.py:212
  101.5 1.6 %collective-permute-done.17 = bf16[128,128]{1,0:T(8,128)(2,1)S(1)} collective-permute-done((bf16[128,128]{1,0:T(8,128)(2,1)S(1)}, bf16[128,128]{1,0:T(8,128)(2,1)S(1)}, u32[]{:S(2)}, u32[]{:S(2)}) %collective-permute-start.17) | collective-permute-done | bytes 32800 | tf_op jit(solution)/shard_map/ppermute | solution.py:212
  103.1 0.6 add_convert_fusion
  (36 shorter events, 4.1 us)
Async XLA Ops:
  0.6 14.6 %copy-start = (bf16[128,1376]{0,1:T(8,128)(2,1)S(1)}, bf16[128,1376]{0,1:T(8,128)(2,1)}, u32[]{:S(2)}) copy-start(bf16[128,1376]{0,1:T(8,128)(2,1)} %param.37) | copy-start | bytes 1056772
  0.6 15.9 %copy-start.1 = (bf16[128,1376]{0,1:T(8,128)(2,1)S(1)}, bf16[128,1376]{0,1:T(8,128)(2,1)}, u32[]{:S(2)}) copy-start(bf16[128,1376]{0,1:T(8,128)(2,1)} %param.38) | copy-start | bytes 1056772
  3.2 31.8 %all-to-all-start = ((bf16[32,4,896]{2,1,0:T(4,128)(2,1)}), bf16[32,4,896]{2,1,0:T(4,128)(2,1)S(1)}, u32[]{:S(2)}, u32[]{:S(2)}) async-start(bf16[32,4,896]{2,1,0:T(4,128)(2,1)} %get-tuple-element.16), calls=%async_computation | async-start | bytes 458752 | tf_op jit(solution)/shard_map/all_to_all | solution.py:228
  15.3 17.1 %collective-permute-start.7 = (bf16[1376,128]{1,0:T(8,128)(2,1)S(1)}, bf16[1376,128]{1,0:T(8,128)(2,1)S(1)}, u32[]{:S(2)}, u32[]{:S(2)}) collective-permute-start(bf16[1376,128]{1,0:T(8,128)(2,1)S(1)} %bitcast.25), channel_id=1, source_target_pairs={{0,8},{8,16},{16,24},{24,0},{1,9},{9,17},{17,25},{25,1},{2,10},{10... | collective-permute-start | bytes 1056776 | tf_op jit(solution)/shard_map/ppermute | solution.py:212
  16.6 17.6 %collective-permute-start.11 = (bf16[1376,128]{1,0:T(8,128)(2,1)S(1)}, bf16[1376,128]{1,0:T(8,128)(2,1)S(1)}, u32[]{:S(2)}, u32[]{:S(2)}) collective-permute-start(bf16[1376,128]{1,0:T(8,128)(2,1)S(1)} %bitcast.28), channel_id=1, source_target_pairs={{0,24},{8,0},{16,8},{24,16},{1,25},{9,1},{17,9},{25,17},{2,26},{10... | collective-permute-start | bytes 1056776 | tf_op jit(solution)/shard_map/ppermute | solution.py:212
  18.0 12.7 %collective-permute-start.2 = (bf16[400,128]{1,0:T(8,128)(2,1)S(1)}, bf16[400,128]{1,0:T(8,128)(2,1)S(1)}, u32[]{:S(2)}, u32[]{:S(2)}) collective-permute-start(bf16[400,128]{1,0:T(8,128)(2,1)S(1)} %get-tuple-element.22.refs_1_.refs_4_), channel_id=1, source_target_pairs={{0,16},{8,24},{16,0},{24,8},{1,17},{9,25},{17,1},{25,9},{2,18},{10... | collective-permute-start | bytes 307208 | tf_op jit(solution)/shard_map/ppermute | solution.py:212
  19.6 12.5 %collective-permute-start.1 = (bf16[400,128]{1,0:T(8,128)(2,1)S(1)}, bf16[400,128]{1,0:T(8,128)(2,1)S(1)}, u32[]{:S(2)}, u32[]{:S(2)}) collective-permute-start(bf16[400,128]{1,0:T(8,128)(2,1)S(1)} %get-tuple-element.22.refs_1_.refs_4_), channel_id=1, source_target_pairs={{0,24},{8,0},{16,8},{24,16},{1,25},{9,1},{17,9},{25,17},{2,26},{10... | collective-permute-start | bytes 307208 | tf_op jit(solution)/shard_map/ppermute | solution.py:212
  20.5 30.3 %collective-permute-start = (bf16[400,128]{1,0:T(8,128)(2,1)S(1)}, bf16[400,128]{1,0:T(8,128)(2,1)S(1)}, u32[]{:S(2)}, u32[]{:S(2)}) collective-permute-start(bf16[400,128]{1,0:T(8,128)(2,1)S(1)} %get-tuple-element.22.refs_1_.refs_4_), channel_id=1, source_target_pairs={{0,8},{8,16},{16,24},{24,0},{1,9},{9,17},{17,25},{25,1},{2,10},{10... | collective-permute-start | bytes 307208 | tf_op jit(solution)/shard_map/ppermute | solution.py:212
  30.8 27.6 %collective-permute-start.8 = (bf16[1376,128]{1,0:T(8,128)(2,1)S(1)}, bf16[1376,128]{1,0:T(8,128)(2,1)S(1)}, u32[]{:S(2)}, u32[]{:S(2)}) collective-permute-start(bf16[1376,128]{1,0:T(8,128)(2,1)S(1)} %bitcast.26), channel_id=1, source_target_pairs={{0,24},{8,0},{16,8},{24,16},{1,25},{9,1},{17,9},{25,17},{2,26},{10... | collective-permute-start | bytes 1056776 | tf_op jit(solution)/shard_map/ppermute | solution.py:212
  32.1 27.1 %collective-permute-start.10 = (bf16[1376,128]{1,0:T(8,128)(2,1)S(1)}, bf16[1376,128]{1,0:T(8,128)(2,1)S(1)}, u32[]{:S(2)}, u32[]{:S(2)}) collective-permute-start(bf16[1376,128]{1,0:T(8,128)(2,1)S(1)} %bitcast.29), channel_id=1, source_target_pairs={{0,8},{8,16},{16,24},{24,0},{1,9},{9,17},{17,25},{25,1},{2,10},{10... | collective-permute-start | bytes 1056776 | tf_op jit(solution)/shard_map/ppermute | solution.py:212
  32.3 30.8 %collective-permute-start.9 = (bf16[1376,128]{1,0:T(8,128)(2,1)S(1)}, bf16[1376,128]{1,0:T(8,128)(2,1)S(1)}, u32[]{:S(2)}, u32[]{:S(2)}) collective-permute-start(bf16[1376,128]{1,0:T(8,128)(2,1)S(1)} %collective-permute-done.7.refs_9_), channel_id=1, source_target_pairs={{0,8},{8,16},{16,24},{24,0},{1,9},{9,17},{17,25},{25,1},{2,10},{10... | collective-permute-start | bytes 1056776 | tf_op jit(solution)/shard_map/ppermute | solution.py:212
  34.2 29.0 %collective-permute-start.12 = (bf16[1376,128]{1,0:T(8,128)(2,1)S(1)}, bf16[1376,128]{1,0:T(8,128)(2,1)S(1)}, u32[]{:S(2)}, u32[]{:S(2)}) collective-permute-start(bf16[1376,128]{1,0:T(8,128)(2,1)S(1)} %collective-permute-done.11.refs_14_), channel_id=1, source_target_pairs={{0,24},{8,0},{16,8},{24,16},{1,25},{9,1},{17,9},{25,17},{2,26},{10... | collective-permute-start | bytes 1056776 | tf_op jit(solution)/shard_map/ppermute | solution.py:212
  50.9 4.6 %collective-permute-start.3 = (bf16[32,512]{1,0:T(8,128)(2,1)S(1)}, bf16[32,512]{1,0:T(8,128)(2,1)S(1)}, u32[]{:S(2)}, u32[]{:S(2)}) collective-permute-start(bf16[32,512]{1,0:T(8,128)(2,1)S(1)} %shard_map.212), channel_id=1, source_target_pairs={{0,1},{1,0},{2,3},{3,2},{4,5},{5,4},{6,7},{7,6},{8,9},{9,8},{10,11... | collective-permute-start | bytes 98312 | tf_op jit(solution)/shard_map/ppermute | solution.py:212
  55.5 4.4 %collective-permute-start.6 = (bf16[32,512]{1,0:T(8,128)(2,1)S(1)}, bf16[32,512]{1,0:T(8,128)(2,1)S(1)}, u32[]{:S(2)}, u32[]{:S(2)}) collective-permute-start(bf16[32,512]{1,0:T(8,128)(2,1)S(1)} %add_convert_fusion.2.refs_0_), channel_id=1, source_target_pairs={{0,4},{2,6},{4,0},{6,2},{1,5},{3,7},{5,1},{7,3},{8,12},{10,14},{12... | collective-permute-start | bytes 98312 | tf_op jit(solution)/shard_map/ppermute | solution.py:212
  58.3 2.8 %collective-permute-start.5 = (bf16[32,512]{1,0:T(8,128)(2,1)S(1)}, bf16[32,512]{1,0:T(8,128)(2,1)S(1)}, u32[]{:S(2)}, u32[]{:S(2)}) collective-permute-start(bf16[32,512]{1,0:T(8,128)(2,1)S(1)} %add_convert_fusion.2.refs_0_), channel_id=1, source_target_pairs={{0,6},{2,0},{4,2},{6,4},{1,7},{3,1},{5,3},{7,5},{8,14},{10,8},{12,... | collective-permute-start | bytes 98312 | tf_op jit(solution)/shard_map/ppermute | solution.py:212
  59.2 4.0 %collective-permute-start.4 = (bf16[32,512]{1,0:T(8,128)(2,1)S(1)}, bf16[32,512]{1,0:T(8,128)(2,1)S(1)}, u32[]{:S(2)}, u32[]{:S(2)}) collective-permute-start(bf16[32,512]{1,0:T(8,128)(2,1)S(1)} %add_convert_fusion.2.refs_0_), channel_id=1, source_target_pairs={{0,2},{2,4},{4,6},{6,0},{1,3},{3,5},{5,7},{7,1},{8,10},{10,12},{12... | collective-permute-start | bytes 98312 | tf_op jit(solution)/shard_map/ppermute | solution.py:212
  76.0 15.3 %all-to-all-start.3 = ((bf16[32,4,1408]{2,1,0:T(4,128)(2,1)}), bf16[32,4,1408]{2,1,0:T(4,128)(2,1)S(1)}, u32[]{:S(2)}, u32[]{:S(2)}) async-start(bf16[32,4,1408]{2,1,0:T(4,128)(2,1)} %broadcast_in_dim.39), calls=%async_computation.3 | async-start | bytes 720896 | tf_op jit(solution)/shard_map/all_to_all | solution.py:223
  79.9 11.5 %collective-permute-start.15 = (bf16[32,128]{1,0:T(8,128)(2,1)S(1)}, bf16[32,128]{1,0:T(8,128)(2,1)S(1)}, u32[]{:S(2)}, u32[]{:S(2)}) collective-permute-start(bf16[32,128]{1,0:T(8,128)(2,1)S(1)} %get-tuple-element.29), channel_id=1, source_target_pairs={{0,16},{8,24},{16,0},{24,8},{1,17},{9,25},{17,1},{25,9},{2,18},{10... | collective-permute-start | bytes 24584 | tf_op jit(solution)/shard_map/ppermute | solution.py:212
  82.8 8.7 %collective-permute-start.14 = (bf16[32,128]{1,0:T(8,128)(2,1)S(1)}, bf16[32,128]{1,0:T(8,128)(2,1)S(1)}, u32[]{:S(2)}, u32[]{:S(2)}) collective-permute-start(bf16[32,128]{1,0:T(8,128)(2,1)S(1)} %get-tuple-element.30), channel_id=1, source_target_pairs={{0,24},{8,0},{16,8},{24,16},{1,25},{9,1},{17,9},{25,17},{2,26},{10... | collective-permute-start | bytes 24584 | tf_op jit(solution)/shard_map/ppermute | solution.py:212
  83.7 7.8 %copy-start.2 = (bf16[1376,128]{1,0:T(8,128)(2,1)S(1)}, bf16[1376,128]{1,0:T(8,128)(2,1)}, u32[]{:S(2)}) copy-start(bf16[1376,128]{1,0:T(8,128)(2,1)} %refs_1_.1) | copy-start | bytes 1056772
  83.7 7.8 %collective-permute-start.13 = (bf16[32,128]{1,0:T(8,128)(2,1)S(1)}, bf16[32,128]{1,0:T(8,128)(2,1)S(1)}, u32[]{:S(2)}, u32[]{:S(2)}) collective-permute-start(bf16[32,128]{1,0:T(8,128)(2,1)S(1)} %get-tuple-element.31), channel_id=1, source_target_pairs={{0,8},{8,16},{16,24},{24,0},{1,9},{9,17},{17,25},{25,1},{2,10},{10... | collective-permute-start | bytes 24584 | tf_op jit(solution)/shard_map/ppermute | solution.py:212
  91.7 5.5 %collective-permute-start.16 = (bf16[128,128]{1,0:T(8,128)(2,1)S(1)}, bf16[128,128]{1,0:T(8,128)(2,1)S(1)}, u32[]{:S(2)}, u32[]{:S(2)}) collective-permute-start(bf16[128,128]{1,0:T(8,128)(2,1)S(1)} %get-tuple-element.26), channel_id=1, source_target_pairs={{0,1},{1,0},{2,3},{3,2},{4,5},{5,4},{6,7},{7,6},{8,9},{9,8},{10,11... | collective-permute-start | bytes 98312 | tf_op jit(solution)/shard_map/ppermute | solution.py:212
  97.3 3.1 %collective-permute-start.19 = (bf16[128,128]{1,0:T(8,128)(2,1)S(1)}, bf16[128,128]{1,0:T(8,128)(2,1)S(1)}, u32[]{:S(2)}, u32[]{:S(2)}) collective-permute-start(bf16[128,128]{1,0:T(8,128)(2,1)S(1)} %add_convert_fusion.1), channel_id=1, source_target_pairs={{0,6},{2,0},{4,2},{6,4},{1,7},{3,1},{5,3},{7,5},{8,14},{10,8},{12,... | collective-permute-start | bytes 98312 | tf_op jit(solution)/shard_map/ppermute | solution.py:212
  97.5 4.0 %collective-permute-start.18 = (bf16[128,128]{1,0:T(8,128)(2,1)S(1)}, bf16[128,128]{1,0:T(8,128)(2,1)S(1)}, u32[]{:S(2)}, u32[]{:S(2)}) collective-permute-start(bf16[128,128]{1,0:T(8,128)(2,1)S(1)} %add_convert_fusion.1), channel_id=1, source_target_pairs={{0,2},{2,4},{4,6},{6,0},{1,3},{3,5},{5,7},{7,1},{8,10},{10,12},{12... | collective-permute-start | bytes 98312 | tf_op jit(solution)/shard_map/ppermute | solution.py:212
  98.8 4.3 %collective-permute-start.17 = (bf16[128,128]{1,0:T(8,128)(2,1)S(1)}, bf16[128,128]{1,0:T(8,128)(2,1)S(1)}, u32[]{:S(2)}, u32[]{:S(2)}) collective-permute-start(bf16[128,128]{1,0:T(8,128)(2,1)S(1)} %add_convert_fusion.1), channel_id=1, source_target_pairs={{0,4},{2,6},{4,0},{6,2},{1,5},{3,7},{5,1},{7,3},{8,12},{10,14},{12... | collective-permute-start | bytes 98312 | tf_op jit(solution)/shard_map/ppermute | solution.py:212

commit v4 on v3

--- a/solution.py
+++ b/solution.py
@@ -184,12 +184,17 @@
         store_shares(out_ref, low, high, at)
 
 
-def hidden_body(got_ref, out_ref):
+def hidden_body(got_ref, out_ref, one_ref, sems):
     total = jnp.sum(got_ref[...].astype(F32), axis=0)
     inv = lax.rsqrt(total[0:4, UNITS : UNITS + 1] / WIDTH + EPS)
     gate = total[0:4] * inv
     up = pltpu.roll(total, 4, 0)[0:4] * inv
-    out_ref[...] = (gate / (1.0 + jnp.exp(-gate)) * up).astype(BF16)
+    one_ref[...] = (gate / (1.0 + jnp.exp(-gate)) * up).astype(BF16)
+    copies = [pltpu.make_async_copy(one_ref, out_ref.at[k], sems.at[k]) for k in range(32)]
+    for copy in copies:
+        copy.start()
+    for copy in copies:
+        copy.wait()
 
 
 def down_body(hidden_ref, down_ref, *refs):
@@ -292,11 +297,18 @@
     middle, second = kernel(
         lift_body, [((4, 32, 128), BF16), ((4, 2, 8, SECOND), BF16)], (*tp_parts(attended), *sent, *gates, *ups)
     )
-    (hidden,) = kernel(hidden_body, [((seqs, SECOND), BF16)], (shares(second.reshape(8, 8, SECOND), "z"),))
+    hidden = pl.pallas_call(
+        hidden_body,
+        out_shape=jax.ShapeDtypeStruct((32, seqs, SECOND), BF16),
+        in_specs=[pl.BlockSpec(memory_space=pltpu.VMEM)],
+        out_specs=pl.BlockSpec(memory_space=pl.ANY),
+        scratch_shapes=[pltpu.VMEM((seqs, SECOND), BF16), pltpu.SemaphoreType.DMA((32,))],
+        compiler_params=pltpu.CompilerParams(vmem_limit_bytes=8 << 20),
+        name="hidden",
+    )(shares(second.reshape(8, 8, SECOND), "z"))
+    hidden = shares(hidden, KV).reshape(32 * seqs, SECOND)
     middles = (middle[0], moved(middle[2], "y", 1), moved(middle[1], "y", 3), moved(middle[3], "y", 2))
-    lifted, middle = kernel(
-        down_body, [((128, 128), BF16), ((128, 128), BF16)], (to_all(hidden, KV), down_weight, *middles)
-    )
+    lifted, middle = kernel(down_body, [((128, 128), BF16), ((128, 128), BF16)], (hidden, down_weight, *middles))
     mine, after, before, across = (part.astype(F32) for part in tp_parts(lifted))
     layer_out = (middle.astype(F32) + ((mine + across) + (after + before))).astype(BF16)
     return (layer_out, new_keys[:, None], new_values[:, None])

time: 104 us -> 104 us (level)
    all_to_all x1 -> x0, waiting for transfers between devices: 7.09 us -> none  [to_all(): got = lax.all_to_all(copies, axes, 0, 0, tiled=True)]
    all_to_all x1 -> x2, waiting for transfers between devices: 0.01 us -> 7.09 us  [shares(): return lax.all_to_all(x, axes, 0, 0, tiled=True)]
    all_to_all x1 -> x2, starting transfers between devices: 12 us -> 15.9 us  [shares(): return lax.all_to_all(x, axes, 0, 0, tiled=True)]
    all_to_all x1 -> x0, starting transfers between devices: 3.88 us -> none  [to_all(): got = lax.all_to_all(copies, axes, 0, 0, tiled=True)]
    pallas_call x0 -> x1, Pallas kernels: none -> 1.14 us  [layer(): pl.pallas_call(hidden_body, out_shape=jax.ShapeDtypeStruct((32, seqs, SEC...]
    pallas_call x5 -> x4, Pallas kernels: 4.07 us -> 3.96 us  [kernel(): pl.pallas_call(whole, out_shape=tuple((pltpu.VMEM(*out) for out in outs))...]
where the time goes in v4:
time: 104 us
  starting transfers between devices  44.8 us (43%)
  blocking collectives  24.8 us (24%)
  waiting for transfers between devices  24.7 us (24%)
  Pallas kernels  6.86 us (7%)
  local copies, waits for them, and re-layouts  1.26 us (1%)
    ppermute x20, starting transfers between devices, moved(): lax.ppermute(x, axis, [(i, (i + shift) % length) for i in range(length)])  28.9 us
    ppermute x20, waiting for transfers between devices, moved(): lax.ppermute(x, axis, [(i, (i + shift) % length) for i in range(length)])  17.6 us
    all_to_all x2, starting transfers between devices, shares(): return lax.all_to_all(x, axes, 0, 0, tiled=True)  15.9 us
    all_to_all x1, blocking collectives, to_all(): got = lax.all_to_all(copies, axes, 0, 0, tiled=True)  13.9 us
    all_to_all x1, blocking collectives, shares(): return lax.all_to_all(x, axes, 0, 0, tiled=True)  10.9 us
    all_to_all x2, waiting for transfers between devices, shares(): return lax.all_to_all(x, axes, 0, 0, tiled=True)  7.09 us
    pallas_call x4, Pallas kernels, kernel(): pl.pallas_call(whole, out_shape=tuple((pltpu.VMEM(*out) for out in outs))...  3.96 us
  transfers between devices with their start and end apart: 22, of which 9 were waited for; matrix products, arithmetic and copies ran while one was open for 1% of the time, Pallas kernels for 2%

profile of v4, /device:TPU:1, one launch (start us, length us, event | category | flops | bytes accessed | tf_op | source)
XLA Modules:
  0.0 103.9 jit_solution(8370154437340656914)
XLA Ops:
  0.7 2.6 %shard_map.211 = (bf16[32,4,896]{2,1,0:T(4,128)(2,1)}, bf16[400,128]{1,0:T(8,128)(2,1)S(1)}, bf16[16,128]{1,0:T(8,128)(2,1)S(1)}, f32[1,128]{1,0:T(1,128)S(1)}, ...) custom-call(bf16[128,128]{1,0:T(8,128)(2,1)} %refs_9_.1, f32[1,128]{1,0:T(1,128)} %bitcast.38, bf16[128,128]{1,0:T(8,128)(2,1)} %refs_2_.1, ...), custom_call_target="tpu_custom_call" | custom-call | tf_op jit(solution)/shard_map/pallas_call | solution.py:44
  3.2 12.0 %all-to-all-start = ((bf16[32,4,896]{2,1,0:T(4,128)(2,1)}), bf16[32,4,896]{2,1,0:T(4,128)(2,1)S(1)}, u32[]{:S(2)}, u32[]{:S(2)}) async-start(bf16[32,4,896]{2,1,0:T(4,128)(2,1)} %get-tuple-element.16), calls=%async_computation | async-start | bytes 458752 | tf_op jit(solution)/shard_map/all_to_all | solution.py:233
  15.3 1.3 %collective-permute-start.7 = (bf16[1376,128]{1,0:T(8,128)(2,1)S(1)}, bf16[1376,128]{1,0:T(8,128)(2,1)S(1)}, u32[]{:S(2)}, u32[]{:S(2)}) collective-permute-start(bf16[1376,128]{1,0:T(8,128)(2,1)S(1)} %bitcast.25), channel_id=1, source_target_pairs={{0,8},{8,16},{16,24},{24,0},{1,9},{9,17},{17,25},{25,1},{2,10},{10... | collective-permute-start | bytes 1056776 | tf_op jit(solution)/shard_map/ppermute | solution.py:217
  16.6 1.4 %collective-permute-start.11 = (bf16[1376,128]{1,0:T(8,128)(2,1)S(1)}, bf16[1376,128]{1,0:T(8,128)(2,1)S(1)}, u32[]{:S(2)}, u32[]{:S(2)}) collective-permute-start(bf16[1376,128]{1,0:T(8,128)(2,1)S(1)} %bitcast.28), channel_id=1, source_target_pairs={{0,24},{8,0},{16,8},{24,16},{1,25},{9,1},{17,9},{25,17},{2,26},{10... | collective-permute-start | bytes 1056776 | tf_op jit(solution)/shard_map/ppermute | solution.py:217
  18.0 1.5 %collective-permute-start.2 = (bf16[400,128]{1,0:T(8,128)(2,1)S(1)}, bf16[400,128]{1,0:T(8,128)(2,1)S(1)}, u32[]{:S(2)}, u32[]{:S(2)}) collective-permute-start(bf16[400,128]{1,0:T(8,128)(2,1)S(1)} %get-tuple-element.22.refs_1_.refs_4_), channel_id=1, source_target_pairs={{0,16},{8,24},{16,0},{24,8},{1,17},{9,25},{17,1},{25,9},{2,18},{10... | collective-permute-start | bytes 307208 | tf_op jit(solution)/shard_map/ppermute | solution.py:217
  19.6 0.9 collective-permute-start.1
  21.0 9.7 %collective-permute-done.2.refs_4_.refs_7_ = bf16[400,128]{1,0:T(8,128)(2,1)S(1)} collective-permute-done((bf16[400,128]{1,0:T(8,128)(2,1)S(1)}, bf16[400,128]{1,0:T(8,128)(2,1)S(1)}, u32[]{:S(2)}, u32[]{:S(2)}) %collective-permute-start.2) | collective-permute-done | bytes 102432 | tf_op jit(solution)/shard_map/ppermute | solution.py:217
  30.8 1.2 %collective-permute-start.8 = (bf16[1376,128]{1,0:T(8,128)(2,1)S(1)}, bf16[1376,128]{1,0:T(8,128)(2,1)S(1)}, u32[]{:S(2)}, u32[]{:S(2)}) collective-permute-start(bf16[1376,128]{1,0:T(8,128)(2,1)S(1)} %bitcast.26), channel_id=1, source_target_pairs={{0,24},{8,0},{16,8},{24,16},{1,25},{9,1},{17,9},{25,17},{2,26},{10... | collective-permute-start | bytes 1056776 | tf_op jit(solution)/shard_map/ppermute | solution.py:217
  32.3 1.9 %collective-permute-start.9 = (bf16[1376,128]{1,0:T(8,128)(2,1)S(1)}, bf16[1376,128]{1,0:T(8,128)(2,1)S(1)}, u32[]{:S(2)}, u32[]{:S(2)}) collective-permute-start(bf16[1376,128]{1,0:T(8,128)(2,1)S(1)} %collective-permute-done.7.refs_9_), channel_id=1, source_target_pairs={{0,8},{8,16},{16,24},{24,0},{1,9},{9,17},{17,25},{25,1},{2,10},{10... | collective-permute-start | bytes 1056776 | tf_op jit(solution)/shard_map/ppermute | solution.py:217
  34.2 0.8 collective-permute-start.12
  35.0 1.8 %attend.1 = (bf16[4,256]{1,0:T(4,128)(2,1)S(1)}, bf16[4,128]{1,0:T(4,128)(2,1)S(1)}, bf16[4,256]{1,0:T(4,128)(2,1)S(1)}) custom-call(bf16[32,4,896]{2,1,0:T(4,128)(2,1)S(1)} %all-to-all-done.got_ref, bf16[16,128]{1,0:T(8,128)(2,1)S(1)} %get-tuple-element.17.dw_ref, f32[1,128]{1,0:T(1,128)S(1)} %get-tuple-element.18.bias_ref, ...), custom_call_target="tpu_custom_call" | custom-call | tf_op jit(solution)/shard_map/attend/pallas_call | solution.py:281
  36.8 13.9 %all_to_all.20 = bf16[8,4,256]{2,1,0:T(4,128)(2,1)S(1)} all-to-all(bf16[8,4,256]{2,1,0:T(4,128)(2,1)S(1)} %broadcast_in_dim.32), channel_id=1, replica_groups=mesh['z'=8,'y'=4,'x'=4,'c'=2] {'z'}, dimensions={0} | all-to-all | bytes 32768 | tf_op jit(solution)/shard_map/all_to_all | solution.py:228
  50.9 3.7 %collective-permute-start.3 = (bf16[32,512]{1,0:T(8,128)(2,1)S(1)}, bf16[32,512]{1,0:T(8,128)(2,1)S(1)}, u32[]{:S(2)}, u32[]{:S(2)}) collective-permute-start(bf16[32,512]{1,0:T(8,128)(2,1)S(1)} %shard_map.212), channel_id=1, source_target_pairs={{0,1},{1,0},{2,3},{3,2},{4,5},{5,4},{6,7},{7,6},{8,9},{9,8},{10,11... | collective-permute-start | bytes 98312 | tf_op jit(solution)/shard_map/ppermute | solution.py:217
  54.6 0.9 collective-permute-done.3
  55.5 2.8 %collective-permute-start.6 = (bf16[32,512]{1,0:T(8,128)(2,1)S(1)}, bf16[32,512]{1,0:T(8,128)(2,1)S(1)}, u32[]{:S(2)}, u32[]{:S(2)}) collective-permute-start(bf16[32,512]{1,0:T(8,128)(2,1)S(1)} %add_convert_fusion.2.refs_0_), channel_id=1, source_target_pairs={{0,4},{2,6},{4,0},{6,2},{1,5},{3,7},{5,1},{7,3},{8,12},{10,14},{12... | collective-permute-start | bytes 98312 | tf_op jit(solution)/shard_map/ppermute | solution.py:217
  58.3 0.9 collective-permute-start.5
  59.2 0.6 collective-permute-start.4
  59.9 1.2 %collective-permute-done.5.refs_2_ = bf16[32,512]{1,0:T(8,128)(2,1)S(1)} collective-permute-done((bf16[32,512]{1,0:T(8,128)(2,1)S(1)}, bf16[32,512]{1,0:T(8,128)(2,1)S(1)}, u32[]{:S(2)}, u32[]{:S(2)}) %collective-permute-start.5) | collective-permute-done | bytes 32800 | tf_op jit(solution)/shard_map/ppermute | solution.py:217
  61.1 2.1 %collective-permute-done.4.refs_1_ = bf16[32,512]{1,0:T(8,128)(2,1)S(1)} collective-permute-done((bf16[32,512]{1,0:T(8,128)(2,1)S(1)}, bf16[32,512]{1,0:T(8,128)(2,1)S(1)}, u32[]{:S(2)}, u32[]{:S(2)}) %collective-permute-start.4) | collective-permute-done | bytes 32800 | tf_op jit(solution)/shard_map/ppermute | solution.py:217
  63.2 1.0 shard_map.213
  64.2 10.9 %all_to_all.21.got_ref = bf16[8,8,1408]{2,1,0:T(8,128)(2,1)S(1)} all-to-all(bf16[8,8,1408]{2,1,0:T(8,128)(2,1)S(1)} %bitcast.31), channel_id=1, replica_groups=mesh['z'=8,'y'=4,'x'=4,'c'=2] {'z'}, dimensions={0} | all-to-all | bytes 360448 | tf_op jit(solution)/shard_map/all_to_all | solution.py:233
  75.0 1.1 %hidden.1 = bf16[32,4,1408]{2,1,0:T(4,128)(2,1)} custom-call(bf16[8,8,1408]{2,1,0:T(8,128)(2,1)S(1)} %all_to_all.21.got_ref), custom_call_target="tpu_custom_call" | custom-call | tf_op jit(solution)/shard_map/hidden/pallas_call | solution.py:300
  76.2 3.9 %all-to-all-start.3 = ((bf16[32,4,1408]{2,1,0:T(4,128)(2,1)}), bf16[32,4,1408]{2,1,0:T(4,128)(2,1)S(1)}, u32[]{:S(2)}, u32[]{:S(2)}) async-start(bf16[32,4,1408]{2,1,0:T(4,128)(2,1)} %hidden.1), calls=%async_computation.3 | async-start | bytes 720896 | tf_op jit(solution)/shard_map/all_to_all | solution.py:233
  80.1 2.9 %collective-permute-start.15 = (bf16[32,128]{1,0:T(8,128)(2,1)S(1)}, bf16[32,128]{1,0:T(8,128)(2,1)S(1)}, u32[]{:S(2)}, u32[]{:S(2)}) collective-permute-start(bf16[32,128]{1,0:T(8,128)(2,1)S(1)} %get-tuple-element.29), channel_id=1, source_target_pairs={{0,16},{8,24},{16,0},{24,8},{1,17},{9,25},{17,1},{25,9},{2,18},{10... | collective-permute-start | bytes 24584 | tf_op jit(solution)/shard_map/ppermute | solution.py:217
  83.0 0.9 collective-permute-start.14
  84.5 7.1 %all-to-all-done.3 = bf16[32,4,1408]{2,1,0:T(4,128)(2,1)S(1)} async-done(((bf16[32,4,1408]{2,1,0:T(4,128)(2,1)}), bf16[32,4,1408]{2,1,0:T(4,128)(2,1)S(1)}, u32[]{:S(2)}, u32[]{:S(2)}) %all-to-all-start.3) | async-done | bytes 360480 | tf_op jit(solution)/shard_map/all_to_all | solution.py:233
  92.0 4.6 %collective-permute-start.16 = (bf16[128,128]{1,0:T(8,128)(2,1)S(1)}, bf16[128,128]{1,0:T(8,128)(2,1)S(1)}, u32[]{:S(2)}, u32[]{:S(2)}) collective-permute-start(bf16[128,128]{1,0:T(8,128)(2,1)S(1)} %get-tuple-element.26), channel_id=1, source_target_pairs={{0,1},{1,0},{2,3},{3,2},{4,5},{5,4},{6,7},{7,6},{8,9},{9,8},{10,11... | collective-permute-start | bytes 98312 | tf_op jit(solution)/shard_map/ppermute | solution.py:217
  96.6 0.9 collective-permute-done.16
  97.7 1.3 %collective-permute-start.18 = (bf16[128,128]{1,0:T(8,128)(2,1)S(1)}, bf16[128,128]{1,0:T(8,128)(2,1)S(1)}, u32[]{:S(2)}, u32[]{:S(2)}) collective-permute-start(bf16[128,128]{1,0:T(8,128)(2,1)S(1)} %add_convert_fusion.1), channel_id=1, source_target_pairs={{0,2},{2,4},{4,6},{6,0},{1,3},{3,5},{5,7},{7,1},{8,10},{10,12},{12... | collective-permute-start | bytes 98312 | tf_op jit(solution)/shard_map/ppermute | solution.py:217
  100.6 1.1 %collective-permute-done.18 = bf16[128,128]{1,0:T(8,128)(2,1)S(1)} collective-permute-done((bf16[128,128]{1,0:T(8,128)(2,1)S(1)}, bf16[128,128]{1,0:T(8,128)(2,1)S(1)}, u32[]{:S(2)}, u32[]{:S(2)}) %collective-permute-start.18) | collective-permute-done | bytes 32800 | tf_op jit(solution)/shard_map/ppermute | solution.py:217
  101.7 1.6 %collective-permute-done.17 = bf16[128,128]{1,0:T(8,128)(2,1)S(1)} collective-permute-done((bf16[128,128]{1,0:T(8,128)(2,1)S(1)}, bf16[128,128]{1,0:T(8,128)(2,1)S(1)}, u32[]{:S(2)}, u32[]{:S(2)}) %collective-permute-start.17) | collective-permute-done | bytes 32800 | tf_op jit(solution)/shard_map/ppermute | solution.py:217
  103.3 0.6 add_convert_fusion
  (35 shorter events, 4.0 us)
Async XLA Ops:
  0.6 14.6 %copy-start = (bf16[128,1376]{0,1:T(8,128)(2,1)S(1)}, bf16[128,1376]{0,1:T(8,128)(2,1)}, u32[]{:S(2)}) copy-start(bf16[128,1376]{0,1:T(8,128)(2,1)} %param.37) | copy-start | bytes 1056772
  0.6 15.9 %copy-start.1 = (bf16[128,1376]{0,1:T(8,128)(2,1)S(1)}, bf16[128,1376]{0,1:T(8,128)(2,1)}, u32[]{:S(2)}) copy-start(bf16[128,1376]{0,1:T(8,128)(2,1)} %param.38) | copy-start | bytes 1056772
  3.2 31.8 %all-to-all-start = ((bf16[32,4,896]{2,1,0:T(4,128)(2,1)}), bf16[32,4,896]{2,1,0:T(4,128)(2,1)S(1)}, u32[]{:S(2)}, u32[]{:S(2)}) async-start(bf16[32,4,896]{2,1,0:T(4,128)(2,1)} %get-tuple-element.16), calls=%async_computation | async-start | bytes 458752 | tf_op jit(solution)/shard_map/all_to_all | solution.py:233
  15.3 17.1 %collective-permute-start.7 = (bf16[1376,128]{1,0:T(8,128)(2,1)S(1)}, bf16[1376,128]{1,0:T(8,128)(2,1)S(1)}, u32[]{:S(2)}, u32[]{:S(2)}) collective-permute-start(bf16[1376,128]{1,0:T(8,128)(2,1)S(1)} %bitcast.25), channel_id=1, source_target_pairs={{0,8},{8,16},{16,24},{24,0},{1,9},{9,17},{17,25},{25,1},{2,10},{10... | collective-permute-start | bytes 1056776 | tf_op jit(solution)/shard_map/ppermute | solution.py:217
  16.6 17.6 %collective-permute-start.11 = (bf16[1376,128]{1,0:T(8,128)(2,1)S(1)}, bf16[1376,128]{1,0:T(8,128)(2,1)S(1)}, u32[]{:S(2)}, u32[]{:S(2)}) collective-permute-start(bf16[1376,128]{1,0:T(8,128)(2,1)S(1)} %bitcast.28), channel_id=1, source_target_pairs={{0,24},{8,0},{16,8},{24,16},{1,25},{9,1},{17,9},{25,17},{2,26},{10... | collective-permute-start | bytes 1056776 | tf_op jit(solution)/shard_map/ppermute | solution.py:217
  18.0 12.7 %collective-permute-start.2 = (bf16[400,128]{1,0:T(8,128)(2,1)S(1)}, bf16[400,128]{1,0:T(8,128)(2,1)S(1)}, u32[]{:S(2)}, u32[]{:S(2)}) collective-permute-start(bf16[400,128]{1,0:T(8,128)(2,1)S(1)} %get-tuple-element.22.refs_1_.refs_4_), channel_id=1, source_target_pairs={{0,16},{8,24},{16,0},{24,8},{1,17},{9,25},{17,1},{25,9},{2,18},{10... | collective-permute-start | bytes 307208 | tf_op jit(solution)/shard_map/ppermute | solution.py:217
  19.6 12.5 %collective-permute-start.1 = (bf16[400,128]{1,0:T(8,128)(2,1)S(1)}, bf16[400,128]{1,0:T(8,128)(2,1)S(1)}, u32[]{:S(2)}, u32[]{:S(2)}) collective-permute-start(bf16[400,128]{1,0:T(8,128)(2,1)S(1)} %get-tuple-element.22.refs_1_.refs_4_), channel_id=1, source_target_pairs={{0,24},{8,0},{16,8},{24,16},{1,25},{9,1},{17,9},{25,17},{2,26},{10... | collective-permute-start | bytes 307208 | tf_op jit(solution)/shard_map/ppermute | solution.py:217
  20.5 30.3 %collective-permute-start = (bf16[400,128]{1,0:T(8,128)(2,1)S(1)}, bf16[400,128]{1,0:T(8,128)(2,1)S(1)}, u32[]{:S(2)}, u32[]{:S(2)}) collective-permute-start(bf16[400,128]{1,0:T(8,128)(2,1)S(1)} %get-tuple-element.22.refs_1_.refs_4_), channel_id=1, source_target_pairs={{0,8},{8,16},{16,24},{24,0},{1,9},{9,17},{17,25},{25,1},{2,10},{10... | collective-permute-start | bytes 307208 | tf_op jit(solution)/shard_map/ppermute | solution.py:217
  30.8 27.6 %collective-permute-start.8 = (bf16[1376,128]{1,0:T(8,128)(2,1)S(1)}, bf16[1376,128]{1,0:T(8,128)(2,1)S(1)}, u32[]{:S(2)}, u32[]{:S(2)}) collective-permute-start(bf16[1376,128]{1,0:T(8,128)(2,1)S(1)} %bitcast.26), channel_id=1, source_target_pairs={{0,24},{8,0},{16,8},{24,16},{1,25},{9,1},{17,9},{25,17},{2,26},{10... | collective-permute-start | bytes 1056776 | tf_op jit(solution)/shard_map/ppermute | solution.py:217
  32.1 27.1 %collective-permute-start.10 = (bf16[1376,128]{1,0:T(8,128)(2,1)S(1)}, bf16[1376,128]{1,0:T(8,128)(2,1)S(1)}, u32[]{:S(2)}, u32[]{:S(2)}) collective-permute-start(bf16[1376,128]{1,0:T(8,128)(2,1)S(1)} %bitcast.29), channel_id=1, source_target_pairs={{0,8},{8,16},{16,24},{24,0},{1,9},{9,17},{17,25},{25,1},{2,10},{10... | collective-permute-start | bytes 1056776 | tf_op jit(solution)/shard_map/ppermute | solution.py:217
  32.3 30.8 %collective-permute-start.9 = (bf16[1376,128]{1,0:T(8,128)(2,1)S(1)}, bf16[1376,128]{1,0:T(8,128)(2,1)S(1)}, u32[]{:S(2)}, u32[]{:S(2)}) collective-permute-start(bf16[1376,128]{1,0:T(8,128)(2,1)S(1)} %collective-permute-done.7.refs_9_), channel_id=1, source_target_pairs={{0,8},{8,16},{16,24},{24,0},{1,9},{9,17},{17,25},{25,1},{2,10},{10... | collective-permute-start | bytes 1056776 | tf_op jit(solution)/shard_map/ppermute | solution.py:217
  34.2 29.0 %collective-permute-start.12 = (bf16[1376,128]{1,0:T(8,128)(2,1)S(1)}, bf16[1376,128]{1,0:T(8,128)(2,1)S(1)}, u32[]{:S(2)}, u32[]{:S(2)}) collective-permute-start(bf16[1376,128]{1,0:T(8,128)(2,1)S(1)} %collective-permute-done.11.refs_14_), channel_id=1, source_target_pairs={{0,24},{8,0},{16,8},{24,16},{1,25},{9,1},{17,9},{25,17},{2,26},{10... | collective-permute-start | bytes 1056776 | tf_op jit(solution)/shard_map/ppermute | solution.py:217
  50.9 4.6 %collective-permute-start.3 = (bf16[32,512]{1,0:T(8,128)(2,1)S(1)}, bf16[32,512]{1,0:T(8,128)(2,1)S(1)}, u32[]{:S(2)}, u32[]{:S(2)}) collective-permute-start(bf16[32,512]{1,0:T(8,128)(2,1)S(1)} %shard_map.212), channel_id=1, source_target_pairs={{0,1},{1,0},{2,3},{3,2},{4,5},{5,4},{6,7},{7,6},{8,9},{9,8},{10,11... | collective-permute-start | bytes 98312 | tf_op jit(solution)/shard_map/ppermute | solution.py:217
  55.5 4.4 %collective-permute-start.6 = (bf16[32,512]{1,0:T(8,128)(2,1)S(1)}, bf16[32,512]{1,0:T(8,128)(2,1)S(1)}, u32[]{:S(2)}, u32[]{:S(2)}) collective-permute-start(bf16[32,512]{1,0:T(8,128)(2,1)S(1)} %add_convert_fusion.2.refs_0_), channel_id=1, source_target_pairs={{0,4},{2,6},{4,0},{6,2},{1,5},{3,7},{5,1},{7,3},{8,12},{10,14},{12... | collective-permute-start | bytes 98312 | tf_op jit(solution)/shard_map/ppermute | solution.py:217
  58.3 2.8 %collective-permute-start.5 = (bf16[32,512]{1,0:T(8,128)(2,1)S(1)}, bf16[32,512]{1,0:T(8,128)(2,1)S(1)}, u32[]{:S(2)}, u32[]{:S(2)}) collective-permute-start(bf16[32,512]{1,0:T(8,128)(2,1)S(1)} %add_convert_fusion.2.refs_0_), channel_id=1, source_target_pairs={{0,6},{2,0},{4,2},{6,4},{1,7},{3,1},{5,3},{7,5},{8,14},{10,8},{12,... | collective-permute-start | bytes 98312 | tf_op jit(solution)/shard_map/ppermute | solution.py:217
  59.2 4.0 %collective-permute-start.4 = (bf16[32,512]{1,0:T(8,128)(2,1)S(1)}, bf16[32,512]{1,0:T(8,128)(2,1)S(1)}, u32[]{:S(2)}, u32[]{:S(2)}) collective-permute-start(bf16[32,512]{1,0:T(8,128)(2,1)S(1)} %add_convert_fusion.2.refs_0_), channel_id=1, source_target_pairs={{0,2},{2,4},{4,6},{6,0},{1,3},{3,5},{5,7},{7,1},{8,10},{10,12},{12... | collective-permute-start | bytes 98312 | tf_op jit(solution)/shard_map/ppermute | solution.py:217
  76.2 15.4 %all-to-all-start.3 = ((bf16[32,4,1408]{2,1,0:T(4,128)(2,1)}), bf16[32,4,1408]{2,1,0:T(4,128)(2,1)S(1)}, u32[]{:S(2)}, u32[]{:S(2)}) async-start(bf16[32,4,1408]{2,1,0:T(4,128)(2,1)} %hidden.1), calls=%async_computation.3 | async-start | bytes 720896 | tf_op jit(solution)/shard_map/all_to_all | solution.py:233
  80.1 11.5 %collective-permute-start.15 = (bf16[32,128]{1,0:T(8,128)(2,1)S(1)}, bf16[32,128]{1,0:T(8,128)(2,1)S(1)}, u32[]{:S(2)}, u32[]{:S(2)}) collective-permute-start(bf16[32,128]{1,0:T(8,128)(2,1)S(1)} %get-tuple-element.29), channel_id=1, source_target_pairs={{0,16},{8,24},{16,0},{24,8},{1,17},{9,25},{17,1},{25,9},{2,18},{10... | collective-permute-start | bytes 24584 | tf_op jit(solution)/shard_map/ppermute | solution.py:217
  83.0 8.7 %collective-permute-start.14 = (bf16[32,128]{1,0:T(8,128)(2,1)S(1)}, bf16[32,128]{1,0:T(8,128)(2,1)S(1)}, u32[]{:S(2)}, u32[]{:S(2)}) collective-permute-start(bf16[32,128]{1,0:T(8,128)(2,1)S(1)} %get-tuple-element.30), channel_id=1, source_target_pairs={{0,24},{8,0},{16,8},{24,16},{1,25},{9,1},{17,9},{25,17},{2,26},{10... | collective-permute-start | bytes 24584 | tf_op jit(solution)/shard_map/ppermute | solution.py:217
  83.9 7.8 %copy-start.2 = (bf16[1376,128]{1,0:T(8,128)(2,1)S(1)}, bf16[1376,128]{1,0:T(8,128)(2,1)}, u32[]{:S(2)}) copy-start(bf16[1376,128]{1,0:T(8,128)(2,1)} %refs_1_.1) | copy-start | bytes 1056772
  83.9 7.8 %collective-permute-start.13 = (bf16[32,128]{1,0:T(8,128)(2,1)S(1)}, bf16[32,128]{1,0:T(8,128)(2,1)S(1)}, u32[]{:S(2)}, u32[]{:S(2)}) collective-permute-start(bf16[32,128]{1,0:T(8,128)(2,1)S(1)} %get-tuple-element.31), channel_id=1, source_target_pairs={{0,8},{8,16},{16,24},{24,0},{1,9},{9,17},{17,25},{25,1},{2,10},{10... | collective-permute-start | bytes 24584 | tf_op jit(solution)/shard_map/ppermute | solution.py:217
  92.0 5.5 %collective-permute-start.16 = (bf16[128,128]{1,0:T(8,128)(2,1)S(1)}, bf16[128,128]{1,0:T(8,128)(2,1)S(1)}, u32[]{:S(2)}, u32[]{:S(2)}) collective-permute-start(bf16[128,128]{1,0:T(8,128)(2,1)S(1)} %get-tuple-element.26), channel_id=1, source_target_pairs={{0,1},{1,0},{2,3},{3,2},{4,5},{5,4},{6,7},{7,6},{8,9},{9,8},{10,11... | collective-permute-start | bytes 98312 | tf_op jit(solution)/shard_map/ppermute | solution.py:217
  97.5 3.1 %collective-permute-start.19 = (bf16[128,128]{1,0:T(8,128)(2,1)S(1)}, bf16[128,128]{1,0:T(8,128)(2,1)S(1)}, u32[]{:S(2)}, u32[]{:S(2)}) collective-permute-start(bf16[128,128]{1,0:T(8,128)(2,1)S(1)} %add_convert_fusion.1), channel_id=1, source_target_pairs={{0,6},{2,0},{4,2},{6,4},{1,7},{3,1},{5,3},{7,5},{8,14},{10,8},{12,... | collective-permute-start | bytes 98312 | tf_op jit(solution)/shard_map/ppermute | solution.py:217
  97.7 4.0 %collective-permute-start.18 = (bf16[128,128]{1,0:T(8,128)(2,1)S(1)}, bf16[128,128]{1,0:T(8,128)(2,1)S(1)}, u32[]{:S(2)}, u32[]{:S(2)}) collective-permute-start(bf16[128,128]{1,0:T(8,128)(2,1)S(1)} %add_convert_fusion.1), channel_id=1, source_target_pairs={{0,2},{2,4},{4,6},{6,0},{1,3},{3,5},{5,7},{7,1},{8,10},{10,12},{12... | collective-permute-start | bytes 98312 | tf_op jit(solution)/shard_map/ppermute | solution.py:217
  99.0 4.3 %collective-permute-start.17 = (bf16[128,128]{1,0:T(8,128)(2,1)S(1)}, bf16[128,128]{1,0:T(8,128)(2,1)S(1)}, u32[]{:S(2)}, u32[]{:S(2)}) collective-permute-start(bf16[128,128]{1,0:T(8,128)(2,1)S(1)} %add_convert_fusion.1), channel_id=1, source_target_pairs={{0,4},{2,6},{4,0},{6,2},{1,5},{3,7},{5,1},{7,3},{8,12},{10,14},{12... | collective-permute-start | bytes 98312 | tf_op jit(solution)/shard_map/ppermute | solution.py:217
